TPU v7x, 32 devices: a whole 2x2x4 slice. The times are simulated.
32 devices in a mesh: sp: 8 (over z, y), tp: 4 (over x, core).
Axes of the slice: x: 2, y: 2, z: 4, core: 2. Of those that a mesh axis runs over, the one named last changes fastest.
Arguments:
- hidden: bfloat16 [2048, 2048], P('sp'), may hold values from -6 to 6
- cotangent: bfloat16 [2048, 2048], P('sp'), may hold values from -6 to 6
- retained: bfloat16 [2048, 2048], P('sp', 'tp'), may hold values from -6 to 6
- queries: bfloat16 [2048, 1024], P('sp', 'tp'), may hold values from -1.5 to 1.5
- key_rows: bfloat16 [2048, 1024], P('sp', 'tp'), may hold values from -1.5 to 1.5
- value_rows: bfloat16 [2048, 2048], P('sp', 'tp'), may hold values from -0.25 to 0.25
- routes: int32 [2048, 2], P('sp'), may hold values from 0 to 7, all different within a row; in each aligned block of 256 rows (0 to 255, 256 to 511, ...) at most 96 rows name the same one
- route_weight: float32 [2048, 2], P('sp'), may hold values from 0.2 to 1.5
- gate_weight: bfloat16 [8, 2048, 1024], P('sp', None, 'tp'), may hold values from -0.125 to 0.125
- up_weight: bfloat16 [8, 2048, 1024], P('sp', None, 'tp'), may hold values from -0.125 to 0.125
- down_weight: bfloat16 [8, 1024, 2048], P('sp', 'tp'), may hold values from -0.1875 to 0.1875
- out_weight: bfloat16 [2048, 2048], P(None, 'tp'), may hold values from -0.125 to 0.125
Outputs:
- gate_grad: float32 [8, 2048, 1024], P('sp', None, 'tp')
- up_grad: float32 [8, 2048, 1024], P('sp', None, 'tp')
- down_grad: float32 [8, 1024, 2048], P('sp', 'tp')
- proj_grad: float32 [2048, 2048], P('sp', 'tp')
- query_gradient: float32 [2048, 1024], P('sp', 'tp')
- key_gradient: float32 [2048, 1024], P('sp', 'tp')
- value_gradient: float32 [2048, 2048], P('sp', 'tp')
Inputs may be any that keep to these rules, and one draw needn't show every extreme that they name: `routes`: each row names 2 different experts; among the 256 rows of one index of sp no expert is named more than 96 times, a bound that some block reaches.
All inputs are finite; a program needn't handle non-finite values.
Results may differ from a plain program's by a relative error of at most 0.013.
Values may be sent and summed in bfloat16 or wider, within the bound.
No kernel may reach another device: no remote copies, remote signals or barrier semaphores. Data moves between devices by JAX's collectives and lax.ppermute only.
A program may use at most 128 MiB of HBM per device.

v0:
```python
import math

import jax
import jax.numpy as jnp
from jax import lax
from jax.experimental import pallas as pl
from jax.experimental.pallas import tpu as pltpu
from jax.sharding import PartitionSpec as P


H = 4


ROWS = (((0,), (0,)), ((), ()))
COLS = (((1,), (1,)), ((), ()))
F32 = jnp.float32
BF16 = jnp.bfloat16


def head_rates(head_ids, total_tokens):
    ids = head_ids.astype(F32)
    exponent = jnp.where(2 * head_ids < H, -5.0 - ids, -math.log2(total_tokens) - (ids - H // 2))
    log_gamma = jnp.log1p(-jnp.exp2(exponent))
    scale = jnp.sqrt(-jnp.expm1(2.0 * log_gamma))
    return (log_gamma, scale)


def swap(x, axis, bits):
    return lax.ppermute(x, axis, [(i, i ^ bits) for i in range(lax.axis_size(axis))])


def far_first(count):
    return sorted(range(1, count), key=lambda k: (-(k & (count // 2)), k))


def exchange(blocks):
    count = blocks.shape[0]
    got = {k: swap(blocks[k], "sp", k) for k in far_first(count)}
    return [got[k] for k in range(1, count)]


def transpose_blocks(x):
    return lax.all_to_all(x, "sp", split_axis=0, concat_axis=0, tiled=True)


def join_body(own_ref, *refs):
    pieces, out_ref = refs[:-1], refs[-1]
    out_ref[0] = own_ref[0]
    for k, piece in enumerate(pieces, 1):
        out_ref[k] = piece[...]


def join(own, pieces):
    (out,) = call(join_body, ((own.shape, own.dtype),), own, *pieces, work=own.size * 256)
    return out


def gather_tp(x):
    pieces = {0: x}
    bit = lax.axis_size("tp") // 2
    while bit:
        pieces.update({k | bit: swap(p, "tp", bit) for k, p in pieces.items()})
        bit //= 2
    return [pieces[k] for k in range(lax.axis_size("tp"))]


def scatter_tp(pieces):
    bit = 1
    pieces = dict(enumerate(pieces))
    while len(pieces) > 1:
        sent = {
            k ^ bit: swap(p.astype(BF16), "tp", bit)
            for k, p in pieces.items()
            if k & bit
        }
        pieces = {k: pieces[k].astype(F32) + sent[k].astype(F32) for k in sent}
        bit *= 2
    return pieces[0]


def flops(count):
    return pl.CostEstimate(flops=int(count), bytes_accessed=0, transcendentals=0)


def call(body, outs, *args, scalars=(), work=0):
    vmem = pl.BlockSpec(memory_space=pltpu.VMEM)
    smem = pl.BlockSpec(memory_space=pltpu.SMEM)
    return pl.pallas_call(
        body,
        in_specs=[smem] * len(scalars) + [vmem] * len(args),
        out_specs=[vmem] * len(outs),
        out_shape=[jax.ShapeDtypeStruct(shape, kind) for shape, kind in outs],
        cost_estimate=flops(work),
    )(*scalars, *args)


def layer_body(pick_ref, own_ref, *refs):
    pieces, (cot_ref, layer_ref) = refs[:-2], refs[-2:]
    total = dot(pick_ref[0], own_ref[0], ROWS)
    for k, piece in enumerate(pieces, 1):
        total = total + dot(pick_ref[k], piece[...], ROWS)
    layer_ref[...] = (cot_ref[...].astype(F32) + total).astype(BF16)


def mix_body(place_ref, *refs):
    pieces, (weight_ref, query_ref, send_ref, mixed_ref, state_ref) = refs[:-5], refs[-5:]
    place = place_ref[0]
    cols = pieces[0].shape[1]
    half = send_ref.shape[2]
    count = send_ref.shape[0] // len(pieces)
    total = None
    for k, piece in enumerate(pieces):
        block = place ^ k
        x = piece[...]
        for q in range(count):
            low = x[:, 2 * q * half : (2 * q + 1) * half]
            high = x[:, (2 * q + 1) * half : (2 * q + 2) * half]
            send_ref[block * count + q] = jnp.where(place % 2 == 0, low, high)
        part = dot(x, weight_ref[pl.ds(block * cols, cols), :])
        total = part if total is None else total + part
    mixed = total.astype(BF16)
    mixed_ref[...] = mixed
    state_ref[...] = dot(query_ref[...], mixed, ROWS).astype(BF16)


def decays(rates_ref, count):
    place = lax.broadcasted_iota(jnp.int32, (count, 1), 0).astype(F32)
    leading = rates_ref[1] * jnp.exp(rates_ref[0] * place)
    trailing = rates_ref[1] * jnp.exp(rates_ref[0] * (count - 1.0 - place))
    return leading, trailing


def paired(low, own_ref, got_ref):
    own, got = own_ref[...], got_ref[...]
    return jnp.concatenate([jnp.where(low, own, got), jnp.where(low, got, own)])


def near_body(ids_ref, rates_ref, mixed_ref, query_ref, key_ref, value_ref, own_ref, got_ref, *outs):
    count = mixed_ref.shape[0]
    mixed, query, key = mixed_ref[...], query_ref[...], key_ref[...]
    row = lax.broadcasted_iota(jnp.int32, (count, count), 0)
    col = lax.broadcasted_iota(jnp.int32, (count, count), 1)
    gap = (row - col).astype(F32)
    weight = rates_ref[1] * jnp.exp(rates_ref[0] * jnp.maximum(gap, 0.0))
    weight = jnp.where(gap >= 0.0, weight, 0.0)
    near_dv = (dot(mixed, value_ref[...], COLS) * weight).astype(BF16)
    near_qk = (dot(query, key, COLS) * weight).astype(BF16)
    prior = paired(ids_ref[1] % 2 == 0, own_ref, got_ref)
    leading, _ = decays(rates_ref, count)
    query_ref, key_near_ref, value_near_ref = outs
    query_ref[...] = dot(near_dv, key) + leading * dot(mixed, prior, COLS)
    key_near_ref[...] = dot(near_dv, query, ROWS)
    value_near_ref[...] = dot(near_qk, mixed, ROWS)


def last_body(ids_ref, rates_ref, own_ref, got_ref, key_ref, value_ref, kn_ref, vn_ref, kg_ref, vg_ref):
    later = paired(ids_ref[1] % 2 == 0, own_ref, got_ref)
    _, trailing = decays(rates_ref, key_ref.shape[0])
    kg_ref[...] = kn_ref[...] + trailing * dot(value_ref[...], later, COLS)
    vg_ref[...] = vn_ref[...] + trailing * dot(key_ref[...], later)


def pre_body(place_ref, *refs):
    pieces = (len(refs) - 2) // 3
    ins, gates, ups = refs[:pieces], refs[pieces : 2 * pieces], refs[2 * pieces : 3 * pieces]
    refs[-2][...] = sum(dot(x[...], w[...]) for x, w in zip(ins, gates))
    refs[-1][...] = sum(dot(x[...], w[...]) for x, w in zip(ins, ups))


def pre_call(place, ins, gate, up):
    slots, cols = ins[0].shape
    units = gate.shape[1]
    pieces = len(ins)
    step = math.gcd(slots, 256)
    row = lambda width: pl.BlockSpec((step, width), lambda i, s: (i, 0))
    weights = [
        pl.BlockSpec((cols, units), lambda i, s, k=k: (s[0] ^ k, 0)) for k in range(pieces)
    ]
    return pl.pallas_call(
        pre_body,
        grid_spec=pltpu.PrefetchScalarGridSpec(
            num_scalar_prefetch=1,
            grid=(slots // step,),
            in_specs=[row(cols)] * pieces + weights * 2,
            out_specs=[row(units)] * 2,
        ),
        out_shape=[jax.ShapeDtypeStruct((slots, units), F32)] * 2,
        cost_estimate=flops(4 * slots * cols * units * pieces),
    )(place, *ins, *[gate] * pieces, *[up] * pieces)


def grad_body(place_ref, *refs):
    place = place_ref[0]
    pieces = (len(refs) - 6) // 2
    ins, ups = refs[:pieces], refs[pieces : 2 * pieces]
    gate_ref, up_ref, product_ref, gate_out, up_out, down_out = refs[2 * pieces :]
    gate_term, up_term, product = gate_ref[...], up_ref[...], product_ref[...]
    for k in range(pieces):
        x = ins[k][...]
        gate_out[place ^ k] = dot(x, gate_term, ROWS)
        up_out[place ^ k] = dot(x, up_term, ROWS)
    width = ups[0].shape[1]
    total = width * pl.num_programs(0)
    for k in range(pieces):
        start = (place ^ k) * total + pl.program_id(0) * width
        start = pl.multiple_of(start, width)
        down_out[:, pl.ds(start, width)] = dot(product, ups[k][...], ROWS)


def grad_call(place, ins, ups, gate_term, up_term, product):
    slots, cols = ins[0].shape
    units = product.shape[1]
    pieces = len(ins)
    step = math.gcd(cols, 256)
    col = pl.BlockSpec((slots, step), lambda i, s: (0, i))
    whole = pl.BlockSpec((slots, units), lambda i, s: (0, 0))
    out = pl.BlockSpec((pieces, step, units), lambda i, s: (0, i, 0))
    gate_grad, up_grad, down_grad = pl.pallas_call(
        grad_body,
        grid_spec=pltpu.PrefetchScalarGridSpec(
            num_scalar_prefetch=1,
            grid=(cols // step,),
            in_specs=[col] * (2 * pieces) + [whole] * 3,
            out_specs=[out, out, pl.BlockSpec((units, pieces * cols), lambda i, s: (0, 0))],
        ),
        out_shape=[jax.ShapeDtypeStruct((pieces, cols, units), F32)] * 2
        + [jax.ShapeDtypeStruct((units, pieces * cols), F32)],
        cost_estimate=flops(6 * slots * cols * units * pieces),
    )(place, *ins, *ups, gate_term, up_term, product)
    width = pieces * cols
    return gate_grad.reshape(width, units), up_grad.reshape(width, units), down_grad


def expert_body(place_ref, *refs):
    ups, downs = refs[0:2], refs[2:4]
    partial_ref, gate_pre_ref, up_pre_ref = refs[4:7]
    outs = (len(refs) - 10) // 3
    gates, upws = refs[7 : 7 + outs], refs[7 + outs : 7 + 2 * outs]
    product_ref, gate_term_ref, up_term_ref = refs[7 + 2 * outs : 10 + 2 * outs]
    rows = refs[10 + 2 * outs :]
    unit_grad = partial_ref[...]
    for x, w in zip(ups, downs):
        unit_grad = unit_grad + dot(x[...], w[...], COLS)
    gate_pre = gate_pre_ref[...]
    up_pre = up_pre_ref[...]
    sigma = jax.nn.sigmoid(gate_pre)
    active = gate_pre * sigma
    product_ref[...] = (active * up_pre).astype(BF16)
    gate_term = (unit_grad * up_pre * sigma * (1.0 + gate_pre * (1.0 - sigma))).astype(BF16)
    up_term = (unit_grad * active).astype(BF16)
    gate_term_ref[...] = gate_term
    up_term_ref[...] = up_term
    for g, u, out in zip(gates, upws, rows):
        out[...] = (dot(gate_term, g[...], COLS) + dot(up_term, u[...], COLS)).astype(BF16)


def expert_call(place, ups, partial, gate_pre, up_pre, down, gate, up):
    slots, cols = ups[0].shape
    units = gate.shape[1]
    pieces = gate.shape[0] // cols
    step = math.gcd(slots, 256)
    row = lambda width: pl.BlockSpec((step, width), lambda i, s: (i, 0))
    down_of = lambda k: pl.BlockSpec((units, cols), lambda i, s, k=k: (0, s[0] ^ k))
    weight_of = lambda k: pl.BlockSpec((cols, units), lambda i, s, k=k: (s[0] ^ k, 0))
    weights = [weight_of(k) for k in range(pieces)]
    return pl.pallas_call(
        expert_body,
        grid_spec=pltpu.PrefetchScalarGridSpec(
            num_scalar_prefetch=1,
            grid=(slots // step,),
            in_specs=[row(cols)] * 2
            + [down_of(pieces - 2), down_of(pieces - 1)]
            + [row(units)] * 3
            + weights
            + weights,
            out_specs=[row(units)] * 3 + [row(cols)] * pieces,
        ),
        out_shape=[jax.ShapeDtypeStruct((slots, units), BF16)] * 3
        + [jax.ShapeDtypeStruct((slots, cols), BF16)] * pieces,
        cost_estimate=flops(6 * slots * cols * units * pieces),
    )(place, *ups, down, down, partial, gate_pre, up_pre, *[gate] * pieces, *[up] * pieces)


def proj_body(place_ref, mine_ref, theirs_ref, even_ref, odd_ref, out_ref):
    place = place_ref[1]
    core = place_ref[0] % 2
    for rows_ref, slot in ((mine_ref, core), (theirs_ref, 1 - core)):
        total = None
        for k in range(even_ref.shape[0]):
            for kept_ref, low in ((even_ref, 0), (odd_ref, 1)):
                part = dot(rows_ref[place ^ (2 * k + low)], kept_ref[k], ROWS)
                total = part if total is None else total + part
        out_ref[slot] = total


def dot(a, b, dims=None):
    if dims is None:
        return jnp.dot(a, b, preferred_element_type=F32)
    return lax.dot_general(a, b, dims, preferred_element_type=F32)


def carry_pair(state, span, reverse):
    low = lax.axis_index("sp") % 2
    first = (low == 1) if reverse else (low == 0)
    half = state.shape[0] // 2
    mine = lax.dynamic_slice_in_dim(state, low * half, half, 0)
    theirs = swap(lax.dynamic_slice_in_dim(state, (1 - low) * half, half, 0), "sp", 1)
    mine, theirs = mine.astype(F32), theirs.astype(F32)
    early = jnp.where(first, mine, theirs)
    late = jnp.where(first, theirs, mine)
    return early, (late + jnp.exp(span) * early).astype(BF16)


def carry_outer(total, reverse):
    count = lax.axis_size("sp")
    sign = -2 if reverse else 2
    return [
        lax.ppermute(
            total, "sp", [(i, i + sign * d) for i in range(count) if 0 <= i + sign * d < count]
        )
        for d in range(1, count // 2)
    ]


def carry_inner(early, outer, span, reverse):
    low = lax.axis_index("sp") % 2
    first = (low == 1) if reverse else (low == 0)
    ahead = jnp.zeros(early.shape, F32)
    for d, piece in enumerate(outer, 1):
        ahead = ahead + jnp.exp(span * (2 * d - 2)) * piece.astype(F32)
    behind = early + jnp.exp(span) * ahead
    own = jnp.where(first, ahead, behind).astype(BF16)
    return own, jnp.where(first, behind, ahead).astype(BF16)


def local(
    hidden,
    cotangent,
    retained,
    queries,
    key_rows,
    value_rows,
    routes,
    route_weight,
    gate_weight,
    up_weight,
    down_weight,
    out_weight,
):
    sp_count = lax.axis_size("sp")
    tp_count = lax.axis_size("tp")
    sp_place = lax.axis_index("sp")
    tp_place = lax.axis_index("tp")
    tokens, width = hidden.shape
    ids = jnp.stack([tp_place, sp_place])
    rates = jnp.stack(head_rates(tp_place, tokens * sp_count))
    log_gamma = rates[0]
    top = routes.shape[1]
    capacity = 3 * tokens * top // (2 * sp_count)
    slots = sp_count * capacity
    col_width = width // tp_count
    gate, up, down = gate_weight[0], up_weight[0], down_weight[0]

    flat = routes.T.reshape(-1)
    order = jnp.arange(flat.shape[0], dtype=jnp.int32)
    before = (flat[None, :] == flat[:, None]) & (order[None, :] < order[:, None])
    rank = jnp.sum(before.astype(jnp.int32), axis=1)
    target = ((flat ^ sp_place) * capacity + rank).reshape(top, tokens)
    place_of = jnp.arange(slots, dtype=jnp.int32)[:, None]
    picks = [(place_of == target[r][None, :]).astype(BF16) for r in range(top)]
    pick_all = sum(picks[1:], picks[0])
    hid_cols = lax.dynamic_slice_in_dim(hidden, tp_place * col_width, col_width, 1)
    cot_cols = lax.dynamic_slice_in_dim(cotangent, tp_place * col_width, col_width, 1)
    cot_wide = cot_cols.astype(F32)
    upstream = jnp.concatenate(
        [(route_weight[:, r : r + 1] * cot_wide).astype(BF16) for r in range(top)], axis=0
    )
    in_send = dot(pick_all, hid_cols).astype(BF16).reshape(sp_count, capacity, col_width)
    up_send = (
        dot(jnp.concatenate(picks, axis=1), upstream)
        .astype(BF16)
        .reshape(sp_count, capacity, col_width)
    )
    got_in = join(in_send, exchange(in_send)).reshape(slots, col_width)
    got_up = join(up_send, exchange(up_send)).reshape(slots, col_width)
    place = jnp.arange(tokens, dtype=F32)
    span = log_gamma * tokens
    suffix_decay = jnp.exp(log_gamma * (tokens - place))[:, None]
    prefix_decay = jnp.exp(log_gamma * (place + 1.0))[:, None]
    key_decayed = (key_rows.astype(F32) * suffix_decay).astype(BF16)
    query_decayed = (queries.astype(F32) * prefix_decay).astype(BF16)
    prior_state = dot(key_decayed, value_rows, ROWS).astype(BF16)
    prior_early, prior_total = carry_pair(prior_state, span, False)
    ins = gather_tp(got_in)
    ups = gather_tp(got_up)
    kept = [retained] + [swap(retained, "sp", k) for k in range(2, sp_count, 2)]
    prior_outer = carry_outer(prior_total, False)
    blocks = [tp_place ^ k for k in range(tp_count)]
    downs = [lax.dynamic_slice_in_dim(down, b * col_width, col_width, 1) for b in blocks[:-2]]
    gate_pre, up_pre = pre_call(ids, ins, gate, up)
    partial = sum(dot(x, w, COLS) for x, w in zip(ups, downs))
    product, gate_term, up_term, *row_parts = expert_call(
        ids, ups[-2:], partial, gate_pre, up_pre, down, gate, up
    )
    row_grad = scatter_tp(row_parts).astype(BF16)
    row_grad = row_grad.reshape(sp_count, capacity, col_width)
    returned = exchange(row_grad)
    even = jnp.stack(kept)
    odd = swap(even, "sp", 1)
    prior_own, prior_sent = carry_inner(prior_early, prior_outer, span, False)
    prior_got = swap(prior_sent, "sp", 1)
    (layer_cols,) = call(
        layer_body,
        (((tokens, col_width), BF16),),
        pick_all.reshape(sp_count, capacity, tokens),
        row_grad,
        *returned,
        cot_cols,
        work=2 * slots * tokens * col_width,
    )

    gate_grad, up_grad, down_grad = grad_call(
        ids, ins, ups, gate_term, up_term, product
    )

    layers = gather_tp(layer_cols)
    half = width // sp_count // 2
    values = value_rows.shape[1]
    layer_send, mixed_grad, state = call(
        mix_body,
        (
            ((sp_count, tokens, half), BF16),
            ((tokens, values), BF16),
            ((queries.shape[1], values), BF16),
        ),
        *layers,
        out_weight,
        query_decayed,
        scalars=(ids,),
        work=2 * tokens * width * values,
    )

    later_early, later_total = carry_pair(state, span, True)
    later_outer = carry_outer(later_total, True)
    mine = transpose_blocks(layer_send)
    later_own, later_sent = carry_inner(later_early, later_outer, span, True)
    later_got = swap(later_sent, "sp", 1)
    theirs = swap(mine, "tp", 1)
    query_gradient, key_near, value_near = call(
        near_body,
        ((queries.shape, F32), (queries.shape, F32), (value_rows.shape, F32)),
        mixed_grad,
        queries,
        key_rows,
        value_rows,
        prior_own,
        prior_got,
        scalars=(ids, rates),
        work=10 * tokens * tokens * values,
    )
    key_gradient, value_gradient = call(
        last_body,
        ((key_near.shape, F32), (value_near.shape, F32)),
        later_own,
        later_got,
        key_rows,
        value_rows,
        key_near,
        value_near,
        scalars=(ids, rates),
        work=4 * tokens * values * queries.shape[1],
    )
    (proj_grad,) = call(
        proj_body,
        (((2, half, retained.shape[1]), F32),),
        mine,
        theirs,
        even,
        odd,
        scalars=(ids,),
        work=2 * sp_count * tokens * 2 * half * retained.shape[1],
    )
    proj_grad = proj_grad.reshape(2 * half, retained.shape[1])
    return (
        gate_grad[None],
        up_grad[None],
        down_grad[None],
        proj_grad,
        query_gradient,
        key_gradient,
        value_gradient,
    )


def solution(mesh):
    return jax.shard_map(
        local,
        mesh=mesh,
        in_specs=(
            P("sp", None),
            P("sp", None),
            P("sp", "tp"),
            P("sp", "tp"),
            P("sp", "tp"),
            P("sp", "tp"),
            P("sp", None),
            P("sp", None),
            P("sp", None, "tp"),
            P("sp", None, "tp"),
            P("sp", "tp", None),
            P(None, "tp"),
        ),
        out_specs=(
            P("sp", None, "tp"),
            P("sp", None, "tp"),
            P("sp", "tp", None),
            P("sp", "tp"),
            P("sp", "tp"),
            P("sp", "tp"),
            P("sp", "tp"),
        ),
        check_vma=False,
    )
```

profile of v0, /device:TPU:0, one launch (start us, length us, event | category | flops | bytes accessed | tf_op | source)
XLA Modules:
  0.0 241.5 jit_solution(437402093170829861)
XLA Ops:
  0.7 0.8 copy.19
  2.3 3.1 %collective-permute-start = (bf16[96,512]{1,0:T(8,128)(2,1)S(1)}, bf16[96,512]{1,0:T(8,128)(2,1)S(1)}, u32[]{:S(2)}, u32[]{:S(2)}) collective-permute-start(bf16[96,512]{1,0:T(8,128)(2,1)S(1)} %get-tuple-element.73), channel_id=1, source_target_pairs={{0,4},{4,0},{8,12},{12,8},{16,20},{20,16},{24,28},{28,24},{1,5},{5... | collective-permute-start | bytes 294920 | tf_op jit(solution)/shard_map/ppermute | solution.py:29
  5.4 1.6 collective-permute-start.1
  7.0 3.0 %collective-permute-start.3 = (bf16[96,512]{1,0:T(8,128)(2,1)S(1)}, bf16[96,512]{1,0:T(8,128)(2,1)S(1)}, u32[]{:S(2)}, u32[]{:S(2)}) collective-permute-start(bf16[96,512]{1,0:T(8,128)(2,1)S(1)} %get-tuple-element.70), channel_id=1, source_target_pairs={{0,16},{4,20},{8,24},{12,28},{16,0},{20,4},{24,8},{28,12},{1,17},{... | collective-permute-start | bytes 294920 | tf_op jit(solution)/shard_map/ppermute | solution.py:29
  10.0 1.3 collective-permute-start.4
  11.5 1.1 fusion.6
  13.4 3.7 %collective-permute-start.5 = (bf16[96,512]{1,0:T(8,128)(2,1)S(1)}, bf16[96,512]{1,0:T(8,128)(2,1)S(1)}, u32[]{:S(2)}, u32[]{:S(2)}) collective-permute-start(bf16[96,512]{1,0:T(8,128)(2,1)S(1)} %get-tuple-element.68), channel_id=1, source_target_pairs={{0,24},{4,28},{8,16},{12,20},{16,8},{20,12},{24,0},{28,4},{1,25},{... | collective-permute-start | bytes 294920 | tf_op jit(solution)/shard_map/ppermute | solution.py:29
  17.1 0.8 fusion.31
  17.9 1.7 collective-permute-start.10
  19.6 1.0 collective-permute-start.11
  20.5 4.7 %collective-permute-done.4.refs_4_ = bf16[96,512]{1,0:T(8,128)(2,1)S(1)} collective-permute-done((bf16[96,512]{1,0:T(8,128)(2,1)S(1)}, bf16[96,512]{1,0:T(8,128)(2,1)S(1)}, u32[]{:S(2)}, u32[]{:S(2)}) %collective-permute-start.4) | collective-permute-done | bytes 98336 | tf_op jit(solution)/shard_map/ppermute | solution.py:29
  25.9 2.3 shard_map.171
  28.2 1.5 collective-permute-start.8
  29.7 5.1 %collective-permute-start.13 = (bf16[96,512]{1,0:T(8,128)(2,1)}, bf16[96,512]{1,0:T(8,128)(2,1)S(1)}, u32[]{:S(2)}, u32[]{:S(2)}) collective-permute-start(bf16[96,512]{1,0:T(8,128)(2,1)} %get-tuple-element.63), channel_id=1, source_target_pairs={{0,16},{4,20},{8,24},{12,28},{16,0},{20,4},{24,8},{28,12},{1,17},{... | collective-permute-start | bytes 294920 | tf_op jit(solution)/shard_map/ppermute | solution.py:29
  34.8 0.8 collective-permute-start.14
  35.6 1.0 collective-permute-start.15
  36.6 3.0 %collective-permute-start.16 = (bf16[96,512]{1,0:T(8,128)(2,1)}, bf16[96,512]{1,0:T(8,128)(2,1)}, u32[]{:S(2)}, u32[]{:S(2)}) collective-permute-start(bf16[96,512]{1,0:T(8,128)(2,1)} %get-tuple-element.60), channel_id=1, source_target_pairs={{0,28},{4,24},{8,20},{12,16},{16,12},{20,8},{24,4},{28,0},{1,29},{... | collective-permute-start | bytes 294920 | tf_op jit(solution)/shard_map/ppermute | solution.py:29
  39.6 6.8 %collective-permute-done.13.refs_3_ = bf16[96,512]{1,0:T(8,128)(2,1)S(1)} collective-permute-done((bf16[96,512]{1,0:T(8,128)(2,1)}, bf16[96,512]{1,0:T(8,128)(2,1)S(1)}, u32[]{:S(2)}, u32[]{:S(2)}) %collective-permute-start.13) | collective-permute-done | bytes 98336 | tf_op jit(solution)/shard_map/ppermute | solution.py:29
  46.4 1.8 collective-permute-done.14.refs_4_
  48.8 2.3 shard_map.172
  52.3 17.1 %collective-permute-done.18.refs_0_.refs_6_ = bf16[768,512]{1,0:T(8,128)(2,1)} collective-permute-done((bf16[768,512]{1,0:T(8,128)(2,1)}, bf16[768,512]{1,0:T(8,128)(2,1)}, u32[]{:S(2)}, u32[]{:S(2)}) %collective-permute-start.18) | collective-permute-done | bytes 786464 | tf_op jit(solution)/shard_map/ppermute | solution.py:29
  70.0 1.5 fusion.17
  71.5 1.3 convolution_add_fusion.refs_4_
  72.8 6.2 %shard_map.173 = (f32[768,256]{1,0:T(8,128)}, f32[768,256]{1,0:T(8,128)}) custom-call(s32[2]{0:T(128)} %pad_add_fusion.place_ref.ids_ref, bf16[768,512]{1,0:T(8,128)(2,1)} %bitcast.54, bf16[768,512]{1,0:T(8,128)(2,1)} %collective-permute-done.7.refs_1_, bf16[768,512]{1,0:T(8,128)(2,1)} %collective-permute-done.8.refs_2_, ...), custom_call_target="tpu_custom_call" | custom-call | flops 1610612736 | tf_op jit(solution)/shard_map/pallas_call | solution.py:179
  79.0 7.6 %shard_map.174 = (bf16[768,256]{1,0:T(8,128)(2,1)}, bf16[768,256]{1,0:T(8,128)(2,1)}, bf16[768,256]{1,0:T(8,128)(2,1)}, bf16[768,512]{1,0:T(8,128)(2,1)}, bf16[7...) custom-call(s32[2]{0:T(128)} %pad_add_fusion.place_ref.ids_ref, ...), custom_call_target="tpu_custom_call" | custom-call | flops 2415919104 | tf_op jit(solution)/shard_map/pallas_call | solution.py:266
  87.3 2.0 collective-permute-done.21
  89.3 1.3 add_convert_fusion.1
  91.3 19.3 %collective-permute-done.22 = bf16[768,512]{1,0:T(8,128)(2,1)S(1)} collective-permute-done((bf16[768,512]{1,0:T(8,128)(2,1)S(1)}, bf16[768,512]{1,0:T(8,128)(2,1)S(1)}, u32[]{:S(2)}, u32[]{:S(2)}) %collective-permute-start.22) | collective-permute-done | bytes 786464 | tf_op jit(solution)/shard_map/ppermute | solution.py:29
  110.9 0.7 fusion.30
  111.7 1.4 collective-permute-start.23
  113.1 4.3 %collective-permute-start.24 = (bf16[96,512]{1,0:T(8,128)(2,1)S(1)}, bf16[96,512]{1,0:T(8,128)(2,1)S(1)}, u32[]{:S(2)}, u32[]{:S(2)}) collective-permute-start(bf16[96,512]{1,0:T(8,128)(2,1)S(1)} %get-tuple-element.58), channel_id=1, source_target_pairs={{0,8},{4,12},{8,0},{12,4},{16,24},{20,28},{24,16},{28,20},{1,9},{5... | collective-permute-start | bytes 294920 | tf_op jit(solution)/shard_map/ppermute | solution.py:29
  117.4 2.9 %collective-permute-start.26 = (bf16[96,512]{1,0:T(8,128)(2,1)S(1)}, bf16[96,512]{1,0:T(8,128)(2,1)}, u32[]{:S(2)}, u32[]{:S(2)}) collective-permute-start(bf16[96,512]{1,0:T(8,128)(2,1)S(1)} %get-tuple-element.56), channel_id=1, source_target_pairs={{0,16},{4,20},{8,24},{12,28},{16,0},{20,4},{24,8},{28,12},{1,17},{... | collective-permute-start | bytes 294920 | tf_op jit(solution)/shard_map/ppermute | solution.py:29
  120.3 1.0 collective-permute-start.27
  121.3 2.4 collective-permute-start.28
  123.6 1.5 collective-permute-start.29
  125.2 1.0 fusion.11.pick_ref
  126.5 2.7 %collective-permute-start.35 = (bf16[256,512]{1,0:T(8,128)(2,1)S(1)}, bf16[256,512]{1,0:T(8,128)(2,1)S(1)}, u32[]{:S(2)}, u32[]{:S(2)}) collective-permute-start(bf16[256,512]{1,0:T(8,128)(2,1)S(1)} %copy-done.14), channel_id=1, source_target_pairs={{0,16},{4,20},{8,24},{12,28},{16,0},{20,4},{24,8},{28,12},{1,17},{... | collective-permute-start | bytes 786440 | tf_op jit(solution)/shard_map/ppermute | solution.py:29
  129.2 5.9 %collective-permute-done.27.refs_4_ = bf16[96,512]{1,0:T(8,128)(2,1)} collective-permute-done((bf16[96,512]{1,0:T(8,128)(2,1)S(1)}, bf16[96,512]{1,0:T(8,128)(2,1)}, u32[]{:S(2)}, u32[]{:S(2)}) %collective-permute-start.27) | collective-permute-done | bytes 98336 | tf_op jit(solution)/shard_map/ppermute | solution.py:29
  135.1 2.5 %collective-permute-start.36 = (bf16[256,512]{1,0:T(8,128)(2,1)S(1)}, bf16[256,512]{1,0:T(8,128)(2,1)S(1)}, u32[]{:S(2)}, u32[]{:S(2)}) collective-permute-start(bf16[256,512]{1,0:T(8,128)(2,1)S(1)} %copy-done.14), channel_id=1, source_target_pairs={{0,24},{4,28},{8,16},{12,20},{16,8},{20,12},{24,0},{28,4},{1,25},{... | collective-permute-start | bytes 786440 | tf_op jit(solution)/shard_map/ppermute | solution.py:29
  137.6 3.0 %shard_map.176.refs_0_ = bf16[256,512]{1,0:T(8,128)(2,1)} custom-call(bf16[8,96,256]{2,1,0:T(8,128)(2,1)} %fusion.11.pick_ref, bf16[8,96,512]{2,1,0:T(8,128)(2,1)} %bitcast.52, bf16[96,512]{1,0:T(8,128)(2,1)} %copy-done.24, bf16[96,512]{1,0:T(8,128)(2,1)} %copy-done.25, bf16[96,512]{1,0:T(8,128)(2,1)} %collective-permute-done.25.refs_2_, ...), custom_call_target="tpu_custom_call" | custom-call | flops 201326592 | tf_op jit(solution)/shard_map/pallas_call | solution.py:88
  141.1 0.8 multiply_convert_fusion.1.refs_5_
  141.8 5.3 %collective-permute-done.31.refs_2_ = bf16[256,512]{1,0:T(8,128)(2,1)S(1)} collective-permute-done((bf16[256,512]{1,0:T(8,128)(2,1)}, bf16[256,512]{1,0:T(8,128)(2,1)S(1)}, u32[]{:S(2)}, u32[]{:S(2)}) %collective-permute-start.31) | collective-permute-done | bytes 262176 | tf_op jit(solution)/shard_map/ppermute | solution.py:29
  147.5 1.3 collective-permute-done.32.refs_3_
  148.8 3.6 %shard_map.177 = (bf16[8,256,128]{2,1,0:T(8,128)(2,1)}, bf16[256,512]{1,0:T(8,128)(2,1)}, bf16[256,512]{1,0:T(8,128)(2,1)}) custom-call(s32[2]{0:T(128)} %pad_add_fusion.place_ref.ids_ref, bf16[256,512]{1,0:T(8,128)(2,1)} %shard_map.176.refs_0_, bf16[256,512]{1,0:T(8,128)(2,1)} %copy-done.19, bf16[256,512]{1,0:T(8,128)(2,1)} %copy-done.18, ...), custom_call_target="tpu_custom_call" | custom-call | flops 536870912 | tf_op jit(solution)/shard_map/pallas_call | solution.py:88
  152.3 15.9 %all-to-all-start = ((bf16[8,256,128]{2,1,0:T(8,128)(2,1)}), bf16[8,256,128]{2,1,0:T(8,128)(2,1)S(1)}, u32[]{:S(2)}, u32[]{:S(2)}) async-start(bf16[8,256,128]{2,1,0:T(8,128)(2,1)} %get-tuple-element.39), calls=%async_computation | async-start | bytes 1048576 | tf_op jit(solution)/shard_map/all_to_all | solution.py:43
  169.0 2.0 collective-permute-start.38
  172.7 1.2 pad_maximum_fusion.even_ref
  174.0 2.1 collective-permute-start.43
  176.1 3.7 %collective-permute-done.38 = bf16[128,512]{1,0:T(8,128)(2,1)S(1)} collective-permute-done((bf16[128,512]{1,0:T(8,128)(2,1)}, bf16[128,512]{1,0:T(8,128)(2,1)S(1)}, u32[]{:S(2)}, u32[]{:S(2)}) %collective-permute-start.38) | collective-permute-done | bytes 131104 | tf_op jit(solution)/shard_map/ppermute | solution.py:29
  179.8 3.4 %collective-permute-start.39 = (bf16[128,512]{1,0:T(8,128)(2,1)S(1)}, bf16[128,512]{1,0:T(8,128)(2,1)S(1)}, u32[]{:S(2)}, u32[]{:S(2)}) collective-permute-start(bf16[128,512]{1,0:T(8,128)(2,1)S(1)} %fusion.14), channel_id=1, source_target_pairs={{0,8},{4,12},{8,16},{12,20},{16,24},{20,28},{1,9},{5,13},{9,17},{1... | collective-permute-start | bytes 393224 | tf_op jit(solution)/shard_map/ppermute | solution.py:318
  183.2 4.8 %collective-permute-start.40 = (bf16[128,512]{1,0:T(8,128)(2,1)S(1)}, bf16[128,512]{1,0:T(8,128)(2,1)S(1)}, u32[]{:S(2)}, u32[]{:S(2)}) collective-permute-start(bf16[128,512]{1,0:T(8,128)(2,1)S(1)} %fusion.14), channel_id=1, source_target_pairs={{0,16},{4,20},{8,24},{12,28},{1,17},{5,21},{9,25},{13,29},{2,18},{... | collective-permute-start | bytes 393224 | tf_op jit(solution)/shard_map/ppermute | solution.py:318
  188.0 1.9 collective-permute-start.41
  190.0 14.7 %collective-permute-done.43 = bf16[128,512]{1,0:T(8,128)(2,1)S(1)} collective-permute-done((bf16[128,512]{1,0:T(8,128)(2,1)S(1)}, bf16[128,512]{1,0:T(8,128)(2,1)S(1)}, u32[]{:S(2)}, u32[]{:S(2)}) %collective-permute-start.43) | collective-permute-done | bytes 131104 | tf_op jit(solution)/shard_map/ppermute | solution.py:29
  204.7 1.3 collective-permute-start.44
  206.0 1.3 collective-permute-start.45
  207.4 1.5 collective-permute-start.46
  209.0 2.0 select_convert_fusion.2
  211.0 1.6 collective-permute-done.44
  212.6 8.4 %collective-permute-done.45 = bf16[128,512]{1,0:T(8,128)(2,1)} collective-permute-done((bf16[128,512]{1,0:T(8,128)(2,1)S(1)}, bf16[128,512]{1,0:T(8,128)(2,1)}, u32[]{:S(2)}, u32[]{:S(2)}) %collective-permute-start.45) | collective-permute-done | bytes 131104 | tf_op jit(solution)/shard_map/ppermute | solution.py:318
  221.0 1.8 select_convert_fusion
  223.4 8.2 %shard_map.175 = (f32[4,512,256]{2,1,0:T(8,128)}, f32[4,512,256]{2,1,0:T(8,128)}, f32[256,2048]{1,0:T(8,128)}) custom-call(s32[2]{0:T(128)} %pad_add_fusion.place_ref.ids_ref, bf16[768,512]{1,0:T(8,128)(2,1)} %bitcast.55, bf16[768,512]{1,0:T(8,128)(2,1)} %collective-permute-done.7.refs_1_, bf16[768,512]{1,0:T(8,128)(2,1)} %collective-permute-done.8.refs_2_, ...), custom_call_target="tpu_custom_call" | custom-call | flops 2415919104 | tf_op jit(solution)/shard_map/pallas_call | solution.py:218
  232.2 2.7 %shard_map.179 = (f32[256,256]{1,0:T(8,128)}, f32[256,256]{1,0:T(8,128)}, f32[256,512]{1,0:T(8,128)}) custom-call(s32[2]{0:T(128)} %pad_add_fusion.place_ref.ids_ref, f32[2]{0:T(128)} %pad_maximum_fusion.1.rates_ref, bf16[256,512]{1,0:T(8,128)(2,1)} %get-tuple-element.40.mixed_ref, bf16[256,256]{1,0:T(8,128)(2,1)} %query_ref.1, bf16[256,256]{1,0:T(8,128)(2,1)} %key_ref.3, ...), custom_call_target="tpu_custom_call" | custom-call | flops 335544320 | tf_op jit(solution)/shard_map/pallas_call | solution.py:88
  235.6 2.6 %shard_map.180 = (f32[256,256]{1,0:T(8,128)}, f32[256,512]{1,0:T(8,128)}) custom-call(s32[2]{0:T(128)} %pad_add_fusion.place_ref.ids_ref, f32[2]{0:T(128)} %pad_maximum_fusion.1.rates_ref, bf16[128,512]{1,0:T(8,128)(2,1)} %get-tuple-element.50.own_ref, bf16[128,512]{1,0:T(8,128)(2,1)} %copy-done.20, bf16[256,256]{1,0:T(8,128)(2,1)} %key_ref.3, ...), custom_call_target="tpu_custom_call" | custom-call | flops 134217728 | tf_op jit(solution)/shard_map/pallas_call | solution.py:88
  238.1 3.4 %shard_map.178 = f32[2,128,512]{2,1,0:T(8,128)} custom-call(s32[2]{0:T(128)} %pad_add_fusion.place_ref.ids_ref, bf16[8,256,128]{2,1,0:T(8,128)(2,1)} %copy-done.9, bf16[8,256,128]{2,1,0:T(8,128)(2,1)} %collective-permute-done.33.theirs_ref, bf16[4,256,512]{2,1,0:T(8,128)(2,1)} %copy-done.3, bf16[4,256,512]{2,1,0:T(8,128)(2,1)} %collective-permute-done.37.odd_ref), custom_call_target="tpu_custom_call" | custom-call | flops 536870912 | tf_op jit(solution)/shard_map/pallas_call | solution.py:88
  (158 shorter events, 12.1 us)
Async XLA Ops:
  2.3 11.0 %collective-permute-start = (bf16[96,512]{1,0:T(8,128)(2,1)S(1)}, bf16[96,512]{1,0:T(8,128)(2,1)S(1)}, u32[]{:S(2)}, u32[]{:S(2)}) collective-permute-start(bf16[96,512]{1,0:T(8,128)(2,1)S(1)} %get-tuple-element.73), channel_id=1, source_target_pairs={{0,4},{4,0},{8,12},{12,8},{16,20},{20,16},{24,28},{28,24},{1,5},{5... | collective-permute-start | bytes 294920 | tf_op jit(solution)/shard_map/ppermute | solution.py:29
  5.4 11.6 %collective-permute-start.1 = (bf16[96,512]{1,0:T(8,128)(2,1)S(1)}, bf16[96,512]{1,0:T(8,128)(2,1)S(1)}, u32[]{:S(2)}, u32[]{:S(2)}) collective-permute-start(bf16[96,512]{1,0:T(8,128)(2,1)S(1)} %get-tuple-element.72), channel_id=1, source_target_pairs={{0,8},{4,12},{8,0},{12,4},{16,24},{20,28},{24,16},{28,20},{1,9},{5... | collective-permute-start | bytes 294920 | tf_op jit(solution)/shard_map/ppermute | solution.py:29
  7.0 10.9 %collective-permute-start.2 = (bf16[96,512]{1,0:T(8,128)(2,1)S(1)}, bf16[96,512]{1,0:T(8,128)(2,1)S(1)}, u32[]{:S(2)}, u32[]{:S(2)}) collective-permute-start(bf16[96,512]{1,0:T(8,128)(2,1)S(1)} %get-tuple-element.71), channel_id=1, source_target_pairs={{0,12},{4,8},{8,4},{12,0},{16,28},{20,24},{24,20},{28,16},{1,13},{... | collective-permute-start | bytes 294920 | tf_op jit(solution)/shard_map/ppermute | solution.py:29
  7.0 12.6 %collective-permute-start.3 = (bf16[96,512]{1,0:T(8,128)(2,1)S(1)}, bf16[96,512]{1,0:T(8,128)(2,1)S(1)}, u32[]{:S(2)}, u32[]{:S(2)}) collective-permute-start(bf16[96,512]{1,0:T(8,128)(2,1)S(1)} %get-tuple-element.70), channel_id=1, source_target_pairs={{0,16},{4,20},{8,24},{12,28},{16,0},{20,4},{24,8},{28,12},{1,17},{... | collective-permute-start | bytes 294920 | tf_op jit(solution)/shard_map/ppermute | solution.py:29
  10.0 15.2 %collective-permute-start.4 = (bf16[96,512]{1,0:T(8,128)(2,1)S(1)}, bf16[96,512]{1,0:T(8,128)(2,1)S(1)}, u32[]{:S(2)}, u32[]{:S(2)}) collective-permute-start(bf16[96,512]{1,0:T(8,128)(2,1)S(1)} %get-tuple-element.69), channel_id=1, source_target_pairs={{0,20},{4,16},{8,28},{12,24},{16,4},{20,0},{24,12},{28,8},{1,21},{... | collective-permute-start | bytes 294920 | tf_op jit(solution)/shard_map/ppermute | solution.py:29
  13.4 11.9 %collective-permute-start.5 = (bf16[96,512]{1,0:T(8,128)(2,1)S(1)}, bf16[96,512]{1,0:T(8,128)(2,1)S(1)}, u32[]{:S(2)}, u32[]{:S(2)}) collective-permute-start(bf16[96,512]{1,0:T(8,128)(2,1)S(1)} %get-tuple-element.68), channel_id=1, source_target_pairs={{0,24},{4,28},{8,16},{12,20},{16,8},{20,12},{24,0},{28,4},{1,25},{... | collective-permute-start | bytes 294920 | tf_op jit(solution)/shard_map/ppermute | solution.py:29
  17.0 8.2 %collective-permute-start.6 = (bf16[96,512]{1,0:T(8,128)(2,1)S(1)}, bf16[96,512]{1,0:T(8,128)(2,1)S(1)}, u32[]{:S(2)}, u32[]{:S(2)}) collective-permute-start(bf16[96,512]{1,0:T(8,128)(2,1)S(1)} %get-tuple-element.67), channel_id=1, source_target_pairs={{0,28},{4,24},{8,20},{12,16},{16,12},{20,8},{24,4},{28,0},{1,29},{... | collective-permute-start | bytes 294920 | tf_op jit(solution)/shard_map/ppermute | solution.py:29
  17.9 16.9 %collective-permute-start.10 = (bf16[96,512]{1,0:T(8,128)(2,1)S(1)}, bf16[96,512]{1,0:T(8,128)(2,1)S(1)}, u32[]{:S(2)}, u32[]{:S(2)}) collective-permute-start(bf16[96,512]{1,0:T(8,128)(2,1)S(1)} %get-tuple-element.66), channel_id=1, source_target_pairs={{0,4},{4,0},{8,12},{12,8},{16,20},{20,16},{24,28},{28,24},{1,5},{5... | collective-permute-start | bytes 294920 | tf_op jit(solution)/shard_map/ppermute | solution.py:29
  19.6 16.0 %collective-permute-start.11 = (bf16[96,512]{1,0:T(8,128)(2,1)S(1)}, bf16[96,512]{1,0:T(8,128)(2,1)S(1)}, u32[]{:S(2)}, u32[]{:S(2)}) collective-permute-start(bf16[96,512]{1,0:T(8,128)(2,1)S(1)} %get-tuple-element.65), channel_id=1, source_target_pairs={{0,8},{4,12},{8,0},{12,4},{16,24},{20,28},{24,16},{28,20},{1,9},{5... | collective-permute-start | bytes 294920 | tf_op jit(solution)/shard_map/ppermute | solution.py:29
  25.2 11.4 %collective-permute-start.12 = (bf16[96,512]{1,0:T(8,128)(2,1)}, bf16[96,512]{1,0:T(8,128)(2,1)S(1)}, u32[]{:S(2)}, u32[]{:S(2)}) collective-permute-start(bf16[96,512]{1,0:T(8,128)(2,1)} %get-tuple-element.64), channel_id=1, source_target_pairs={{0,12},{4,8},{8,4},{12,0},{16,28},{20,24},{24,20},{28,16},{1,13},{... | collective-permute-start | bytes 294920 | tf_op jit(solution)/shard_map/ppermute | solution.py:29
  28.2 23.5 %copy-start.4 = (bf16[8,96,512]{2,1,0:T(8,128)(2,1)S(1)}, bf16[8,96,512]{2,1,0:T(8,128)(2,1)}, u32[]{:S(2)}) copy-start(bf16[8,96,512]{2,1,0:T(8,128)(2,1)} %shard_map.171) | copy-start | bytes 2359300
  28.2 41.8 %copy-start.1 = (bf16[1,256,2048]{2,1,0:T(8,128)(2,1)S(1)}, bf16[1,256,2048]{2,1,0:T(8,128)(2,1)}, u32[]{:S(2)}) copy-start(bf16[1,256,2048]{2,1,0:T(8,128)(2,1)} %param.22) | copy-start | bytes 3145732
  28.2 24.0 %collective-permute-start.8 = (bf16[768,512]{1,0:T(8,128)(2,1)}, bf16[768,512]{1,0:T(8,128)(2,1)}, u32[]{:S(2)}, u32[]{:S(2)}) collective-permute-start(bf16[768,512]{1,0:T(8,128)(2,1)} %bitcast.53), channel_id=1, source_target_pairs={{0,2},{1,3},{2,0},{3,1},{4,6},{5,7},{6,4},{7,5},{8,10},{9,11},{10,... | collective-permute-start | bytes 2359304 | tf_op jit(solution)/shard_map/ppermute | solution.py:29
  29.7 16.6 %collective-permute-start.13 = (bf16[96,512]{1,0:T(8,128)(2,1)}, bf16[96,512]{1,0:T(8,128)(2,1)S(1)}, u32[]{:S(2)}, u32[]{:S(2)}) collective-permute-start(bf16[96,512]{1,0:T(8,128)(2,1)} %get-tuple-element.63), channel_id=1, source_target_pairs={{0,16},{4,20},{8,24},{12,28},{16,0},{20,4},{24,8},{28,12},{1,17},{... | collective-permute-start | bytes 294920 | tf_op jit(solution)/shard_map/ppermute | solution.py:29
  34.8 13.4 %copy-start.30 = (bf16[96,512]{1,0:T(8,128)(2,1)}, bf16[96,512]{1,0:T(8,128)(2,1)S(1)}, u32[]{:S(2)}) copy-start(bf16[96,512]{1,0:T(8,128)(2,1)S(1)} %collective-permute-done.10.refs_0_) | copy-start | bytes 294916
  34.8 13.4 %collective-permute-start.14 = (bf16[96,512]{1,0:T(8,128)(2,1)}, bf16[96,512]{1,0:T(8,128)(2,1)S(1)}, u32[]{:S(2)}, u32[]{:S(2)}) collective-permute-start(bf16[96,512]{1,0:T(8,128)(2,1)} %get-tuple-element.62), channel_id=1, source_target_pairs={{0,20},{4,16},{8,28},{12,24},{16,4},{20,0},{24,12},{28,8},{1,21},{... | collective-permute-start | bytes 294920 | tf_op jit(solution)/shard_map/ppermute | solution.py:29
  35.6 12.6 %copy-start.32 = (bf16[96,512]{1,0:T(8,128)(2,1)}, bf16[96,512]{1,0:T(8,128)(2,1)S(1)}, u32[]{:S(2)}) copy-start(bf16[96,512]{1,0:T(8,128)(2,1)S(1)} %collective-permute-done.11.refs_1_) | copy-start | bytes 294916
  35.6 12.5 %collective-permute-start.15 = (bf16[96,512]{1,0:T(8,128)(2,1)}, bf16[96,512]{1,0:T(8,128)(2,1)S(1)}, u32[]{:S(2)}, u32[]{:S(2)}) collective-permute-start(bf16[96,512]{1,0:T(8,128)(2,1)} %get-tuple-element.61), channel_id=1, source_target_pairs={{0,24},{4,28},{8,16},{12,20},{16,8},{20,12},{24,0},{28,4},{1,25},{... | collective-permute-start | bytes 294920 | tf_op jit(solution)/shard_map/ppermute | solution.py:29
  36.6 11.6 %collective-permute-start.16 = (bf16[96,512]{1,0:T(8,128)(2,1)}, bf16[96,512]{1,0:T(8,128)(2,1)}, u32[]{:S(2)}, u32[]{:S(2)}) collective-permute-start(bf16[96,512]{1,0:T(8,128)(2,1)} %get-tuple-element.60), channel_id=1, source_target_pairs={{0,28},{4,24},{8,20},{12,16},{16,12},{20,8},{24,4},{28,0},{1,29},{... | collective-permute-start | bytes 294920 | tf_op jit(solution)/shard_map/ppermute | solution.py:29
  51.2 18.2 %collective-permute-start.18 = (bf16[768,512]{1,0:T(8,128)(2,1)}, bf16[768,512]{1,0:T(8,128)(2,1)}, u32[]{:S(2)}, u32[]{:S(2)}) collective-permute-start(bf16[768,512]{1,0:T(8,128)(2,1)} %bitcast.57), channel_id=1, source_target_pairs={{0,2},{1,3},{2,0},{3,1},{4,6},{5,7},{6,4},{7,5},{8,10},{9,11},{10,... | collective-permute-start | bytes 2359304 | tf_op jit(solution)/shard_map/ppermute | solution.py:29
  51.7 18.3 %collective-permute-start.17 = (bf16[768,512]{1,0:T(8,128)(2,1)}, bf16[768,512]{1,0:T(8,128)(2,1)}, u32[]{:S(2)}, u32[]{:S(2)}) collective-permute-start(bf16[768,512]{1,0:T(8,128)(2,1)} %bitcast.58), channel_id=1, source_target_pairs={{0,1},{1,0},{2,3},{3,2},{4,5},{5,4},{6,7},{7,6},{8,9},{9,8},{10,11... | collective-permute-start | bytes 2359304 | tf_op jit(solution)/shard_map/ppermute | solution.py:29
  51.7 21.1 %collective-permute-start.7 = (bf16[768,512]{1,0:T(8,128)(2,1)S(1)}, bf16[768,512]{1,0:T(8,128)(2,1)}, u32[]{:S(2)}, u32[]{:S(2)}) collective-permute-start(bf16[768,512]{1,0:T(8,128)(2,1)S(1)} %bitcast.56), channel_id=1, source_target_pairs={{0,1},{1,0},{2,3},{3,2},{4,5},{5,4},{6,7},{7,6},{8,9},{9,8},{10,11... | collective-permute-start | bytes 2359304 | tf_op jit(solution)/shard_map/ppermute | solution.py:29
  52.2 20.6 %collective-permute-start.9 = (bf16[768,512]{1,0:T(8,128)(2,1)}, bf16[768,512]{1,0:T(8,128)(2,1)}, u32[]{:S(2)}, u32[]{:S(2)}) collective-permute-start(bf16[768,512]{1,0:T(8,128)(2,1)} %collective-permute-done.8.refs_2_), channel_id=1, source_target_pairs={{0,1},{1,0},{2,3},{3,2},{4,5},{5,4},{6,7},{7,6},{8,9},{9,8},{10,11... | collective-permute-start | bytes 2359304 | tf_op jit(solution)/shard_map/ppermute | solution.py:29
  52.3 19.2 %copy-start.5 = (bf16[8,96,512]{2,1,0:T(8,128)(2,1)S(1)}, bf16[8,96,512]{2,1,0:T(8,128)(2,1)}, u32[]{:S(2)}) copy-start(bf16[8,96,512]{2,1,0:T(8,128)(2,1)} %shard_map.172) | copy-start | bytes 2359300
  69.4 9.7 %collective-permute-start.19 = (bf16[768,512]{1,0:T(8,128)(2,1)}, bf16[768,512]{1,0:T(8,128)(2,1)}, u32[]{:S(2)}, u32[]{:S(2)}) collective-permute-start(bf16[768,512]{1,0:T(8,128)(2,1)} %collective-permute-done.18.refs_0_.refs_6_), channel_id=1, source_target_pairs={{0,1},{1,0},{2,3},{3,2},{4,5},{5,4},{6,7},{7,6},{8,9},{9,8},{10,11... | collective-permute-start | bytes 2359304 | tf_op jit(solution)/shard_map/ppermute | solution.py:29
  86.6 23.9 %copy-start.11 = (bf16[768,512]{1,0:T(8,128)(2,1)S(1)}, bf16[768,512]{1,0:T(8,128)(2,1)}, u32[]{:S(2)}) copy-start(bf16[768,512]{1,0:T(8,128)(2,1)} %get-tuple-element.35) | copy-start | bytes 2359300
  86.6 2.7 %collective-permute-start.21 = (bf16[768,512]{1,0:T(8,128)(2,1)}, bf16[768,512]{1,0:T(8,128)(2,1)S(1)}, u32[]{:S(2)}, u32[]{:S(2)}) collective-permute-start(bf16[768,512]{1,0:T(8,128)(2,1)} %get-tuple-element.38), channel_id=1, source_target_pairs={{0,1},{1,0},{2,3},{3,2},{4,5},{5,4},{6,7},{7,6},{8,9},{9,8},{10,11... | collective-permute-start | bytes 2359304 | tf_op jit(solution)/shard_map/ppermute | solution.py:29
  87.2 4.1 %collective-permute-start.20 = (bf16[768,512]{1,0:T(8,128)(2,1)}, bf16[768,512]{1,0:T(8,128)(2,1)S(1)}, u32[]{:S(2)}, u32[]{:S(2)}) collective-permute-start(bf16[768,512]{1,0:T(8,128)(2,1)} %get-tuple-element.36), channel_id=1, source_target_pairs={{0,1},{1,0},{2,3},{3,2},{4,5},{5,4},{6,7},{7,6},{8,9},{9,8},{10,11... | collective-permute-start | bytes 2359304 | tf_op jit(solution)/shard_map/ppermute | solution.py:29
  90.7 19.9 %collective-permute-start.22 = (bf16[768,512]{1,0:T(8,128)(2,1)S(1)}, bf16[768,512]{1,0:T(8,128)(2,1)S(1)}, u32[]{:S(2)}, u32[]{:S(2)}) collective-permute-start(bf16[768,512]{1,0:T(8,128)(2,1)S(1)} %add_convert_fusion.1), channel_id=1, source_target_pairs={{0,2},{1,3},{2,0},{3,1},{4,6},{5,7},{6,4},{7,5},{8,10},{9,11},{10,... | collective-permute-start | bytes 2359304 | tf_op jit(solution)/shard_map/ppermute | solution.py:29
  110.9 26.7 %copy-start.2 = (bf16[768,512]{1,0:T(8,128)(2,1)}, bf16[768,512]{1,0:T(8,128)(2,1)S(1)}, u32[]{:S(2)}) copy-start(bf16[768,512]{1,0:T(8,128)(2,1)S(1)} %add_convert_fusion) | copy-start | bytes 2359300
  110.9 15.3 %copy-start.14 = (bf16[256,512]{1,0:T(8,128)(2,1)S(1)}, bf16[256,512]{1,0:T(8,128)(2,1)}, u32[]{:S(2)}) copy-start(bf16[256,512]{1,0:T(8,128)(2,1)} %param.14) | copy-start | bytes 786436
  111.7 29.4 %copy-start.21 = (bf16[256,256]{1,0:T(8,128)(2,1)S(1)}, bf16[256,256]{1,0:T(8,128)(2,1)}, u32[]{:S(2)}) copy-start(bf16[256,256]{1,0:T(8,128)(2,1)} %query_ref.1) | copy-start | bytes 393220
  111.7 35.5 %copy-start.10 = (bf16[256,512]{1,0:T(8,128)(2,1)S(1)}, bf16[256,512]{1,0:T(8,128)(2,1)}, u32[]{:S(2)}) copy-start(bf16[256,512]{1,0:T(8,128)(2,1)} %value_ref.3) | copy-start | bytes 786436
  111.7 35.5 %copy-start.13 = (bf16[256,256]{1,0:T(8,128)(2,1)S(1)}, bf16[256,256]{1,0:T(8,128)(2,1)}, u32[]{:S(2)}) copy-start(bf16[256,256]{1,0:T(8,128)(2,1)} %key_ref.3) | copy-start | bytes 393220
  111.7 9.6 %collective-permute-start.23 = (bf16[96,512]{1,0:T(8,128)(2,1)S(1)}, bf16[96,512]{1,0:T(8,128)(2,1)S(1)}, u32[]{:S(2)}, u32[]{:S(2)}) collective-permute-start(bf16[96,512]{1,0:T(8,128)(2,1)S(1)} %get-tuple-element.59), channel_id=1, source_target_pairs={{0,4},{4,0},{8,12},{12,8},{16,20},{20,16},{24,28},{28,24},{1,5},{5... | collective-permute-start | bytes 294920 | tf_op jit(solution)/shard_map/ppermute | solution.py:29
  113.1 10.6 %collective-permute-start.24 = (bf16[96,512]{1,0:T(8,128)(2,1)S(1)}, bf16[96,512]{1,0:T(8,128)(2,1)S(1)}, u32[]{:S(2)}, u32[]{:S(2)}) collective-permute-start(bf16[96,512]{1,0:T(8,128)(2,1)S(1)} %get-tuple-element.58), channel_id=1, source_target_pairs={{0,8},{4,12},{8,0},{12,4},{16,24},{20,28},{24,16},{28,20},{1,9},{5... | collective-permute-start | bytes 294920 | tf_op jit(solution)/shard_map/ppermute | solution.py:29
  117.3 8.9 %collective-permute-start.25 = (bf16[96,512]{1,0:T(8,128)(2,1)S(1)}, bf16[96,512]{1,0:T(8,128)(2,1)}, u32[]{:S(2)}, u32[]{:S(2)}) collective-permute-start(bf16[96,512]{1,0:T(8,128)(2,1)S(1)} %get-tuple-element.57), channel_id=1, source_target_pairs={{0,12},{4,8},{8,4},{12,0},{16,28},{20,24},{24,20},{28,16},{1,13},{... | collective-permute-start | bytes 294920 | tf_op jit(solution)/shard_map/ppermute | solution.py:29
  117.4 9.0 %collective-permute-start.26 = (bf16[96,512]{1,0:T(8,128)(2,1)S(1)}, bf16[96,512]{1,0:T(8,128)(2,1)}, u32[]{:S(2)}, u32[]{:S(2)}) collective-permute-start(bf16[96,512]{1,0:T(8,128)(2,1)S(1)} %get-tuple-element.56), channel_id=1, source_target_pairs={{0,16},{4,20},{8,24},{12,28},{16,0},{20,4},{24,8},{28,12},{1,17},{... | collective-permute-start | bytes 294920 | tf_op jit(solution)/shard_map/ppermute | solution.py:29
  120.3 14.8 %collective-permute-start.27 = (bf16[96,512]{1,0:T(8,128)(2,1)S(1)}, bf16[96,512]{1,0:T(8,128)(2,1)}, u32[]{:S(2)}, u32[]{:S(2)}) collective-permute-start(bf16[96,512]{1,0:T(8,128)(2,1)S(1)} %get-tuple-element.55), channel_id=1, source_target_pairs={{0,20},{4,16},{8,28},{12,24},{16,4},{20,0},{24,12},{28,8},{1,21},{... | collective-permute-start | bytes 294920 | tf_op jit(solution)/shard_map/ppermute | solution.py:29
  121.3 16.3 %copy-start.24 = (bf16[96,512]{1,0:T(8,128)(2,1)}, bf16[96,512]{1,0:T(8,128)(2,1)S(1)}, u32[]{:S(2)}) copy-start(bf16[96,512]{1,0:T(8,128)(2,1)S(1)} %collective-permute-done.23.refs_0_) | copy-start | bytes 294916
  121.3 16.3 %collective-permute-start.28 = (bf16[96,512]{1,0:T(8,128)(2,1)}, bf16[96,512]{1,0:T(8,128)(2,1)}, u32[]{:S(2)}, u32[]{:S(2)}) collective-permute-start(bf16[96,512]{1,0:T(8,128)(2,1)} %get-tuple-element.54), channel_id=1, source_target_pairs={{0,24},{4,28},{8,16},{12,20},{16,8},{20,12},{24,0},{28,4},{1,25},{... | collective-permute-start | bytes 294920 | tf_op jit(solution)/shard_map/ppermute | solution.py:29
  123.6 13.9 %collective-permute-start.29 = (bf16[96,512]{1,0:T(8,128)(2,1)}, bf16[96,512]{1,0:T(8,128)(2,1)}, u32[]{:S(2)}, u32[]{:S(2)}) collective-permute-start(bf16[96,512]{1,0:T(8,128)(2,1)} %get-tuple-element.53), channel_id=1, source_target_pairs={{0,28},{4,24},{8,20},{12,16},{16,12},{20,8},{24,4},{28,0},{1,29},{... | collective-permute-start | bytes 294920 | tf_op jit(solution)/shard_map/ppermute | solution.py:29
  126.3 45.5 %collective-permute-start.34 = (bf16[256,512]{1,0:T(8,128)(2,1)S(1)}, bf16[256,512]{1,0:T(8,128)(2,1)S(1)}, u32[]{:S(2)}, u32[]{:S(2)}) collective-permute-start(bf16[256,512]{1,0:T(8,128)(2,1)S(1)} %copy-done.14), channel_id=1, source_target_pairs={{0,8},{4,12},{8,0},{12,4},{16,24},{20,28},{24,16},{28,20},{1,9},{5... | collective-permute-start | bytes 786440 | tf_op jit(solution)/shard_map/ppermute | solution.py:29
  126.5 45.3 %collective-permute-start.35 = (bf16[256,512]{1,0:T(8,128)(2,1)S(1)}, bf16[256,512]{1,0:T(8,128)(2,1)S(1)}, u32[]{:S(2)}, u32[]{:S(2)}) collective-permute-start(bf16[256,512]{1,0:T(8,128)(2,1)S(1)} %copy-done.14), channel_id=1, source_target_pairs={{0,16},{4,20},{8,24},{12,28},{16,0},{20,4},{24,8},{28,12},{1,17},{... | collective-permute-start | bytes 786440 | tf_op jit(solution)/shard_map/ppermute | solution.py:29
  135.1 36.8 %collective-permute-start.36 = (bf16[256,512]{1,0:T(8,128)(2,1)S(1)}, bf16[256,512]{1,0:T(8,128)(2,1)S(1)}, u32[]{:S(2)}, u32[]{:S(2)}) collective-permute-start(bf16[256,512]{1,0:T(8,128)(2,1)S(1)} %copy-done.14), channel_id=1, source_target_pairs={{0,24},{4,28},{8,16},{12,20},{16,8},{20,12},{24,0},{28,4},{1,25},{... | collective-permute-start | bytes 786440 | tf_op jit(solution)/shard_map/ppermute | solution.py:29
  140.5 6.6 %collective-permute-start.31 = (bf16[256,512]{1,0:T(8,128)(2,1)}, bf16[256,512]{1,0:T(8,128)(2,1)S(1)}, u32[]{:S(2)}, u32[]{:S(2)}) collective-permute-start(bf16[256,512]{1,0:T(8,128)(2,1)} %shard_map.176.refs_0_), channel_id=1, source_target_pairs={{0,2},{1,3},{2,0},{3,1},{4,6},{5,7},{6,4},{7,5},{8,10},{9,11},{10,... | collective-permute-start | bytes 786440 | tf_op jit(solution)/shard_map/ppermute | solution.py:29
  141.8 5.7 %collective-permute-start.30 = (bf16[256,512]{1,0:T(8,128)(2,1)}, bf16[256,512]{1,0:T(8,128)(2,1)S(1)}, u32[]{:S(2)}, u32[]{:S(2)}) collective-permute-start(bf16[256,512]{1,0:T(8,128)(2,1)} %shard_map.176.refs_0_), channel_id=1, source_target_pairs={{0,1},{1,0},{2,3},{3,2},{4,5},{5,4},{6,7},{7,6},{8,9},{9,8},{10,11... | collective-permute-start | bytes 786440 | tf_op jit(solution)/shard_map/ppermute | solution.py:29
  147.1 1.7 collective-permute-start.32
  152.3 21.7 %copy-start.12 = (bf16[256,512]{1,0:T(8,128)(2,1)S(1)}, bf16[256,512]{1,0:T(8,128)(2,1)}, u32[]{:S(2)}) copy-start(bf16[256,512]{1,0:T(8,128)(2,1)} %get-tuple-element.42) | copy-start | bytes 786436
  152.3 56.5 %all-to-all-start = ((bf16[8,256,128]{2,1,0:T(8,128)(2,1)}), bf16[8,256,128]{2,1,0:T(8,128)(2,1)S(1)}, u32[]{:S(2)}, u32[]{:S(2)}) async-start(bf16[8,256,128]{2,1,0:T(8,128)(2,1)} %get-tuple-element.39), calls=%async_computation | async-start | bytes 1048576 | tf_op jit(solution)/shard_map/all_to_all | solution.py:43
  169.0 10.8 %collective-permute-start.38 = (bf16[128,512]{1,0:T(8,128)(2,1)}, bf16[128,512]{1,0:T(8,128)(2,1)S(1)}, u32[]{:S(2)}, u32[]{:S(2)}) collective-permute-start(bf16[128,512]{1,0:T(8,128)(2,1)} %constant_dynamic-slice_fusion.1), channel_id=1, source_target_pairs={{0,4},{4,0},{8,12},{12,8},{16,20},{20,16},{24,28},{28,24},{1,5},{5... | collective-permute-start | bytes 393224 | tf_op jit(solution)/shard_map/ppermute | solution.py:29
  173.9 57.6 %copy-start.3 = (bf16[4,256,512]{2,1,0:T(8,128)(2,1)}, bf16[4,256,512]{2,1,0:T(8,128)(2,1)S(1)}, u32[]{:S(2)}) copy-start(bf16[4,256,512]{2,1,0:T(8,128)(2,1)S(1)} %pad_maximum_fusion.even_ref) | copy-start | bytes 3145732
  173.9 64.2 %collective-permute-start.37 = (bf16[4,256,512]{2,1,0:T(8,128)(2,1)S(1)}, bf16[4,256,512]{2,1,0:T(8,128)(2,1)}, u32[]{:S(2)}, u32[]{:S(2)}) collective-permute-start(bf16[4,256,512]{2,1,0:T(8,128)(2,1)S(1)} %pad_maximum_fusion.even_ref), channel_id=1, source_target_pairs={{0,4},{4,0},{8,12},{12,8},{16,20},{20,16},{24,28},{28,24},{1,5},{5... | collective-permute-start | bytes 3145736 | tf_op jit(solution)/shard_map/ppermute | solution.py:29
  174.0 30.6 %collective-permute-start.43 = (bf16[128,512]{1,0:T(8,128)(2,1)S(1)}, bf16[128,512]{1,0:T(8,128)(2,1)S(1)}, u32[]{:S(2)}, u32[]{:S(2)}) collective-permute-start(bf16[128,512]{1,0:T(8,128)(2,1)S(1)} %constant_dynamic-slice_fusion), channel_id=1, source_target_pairs={{0,4},{4,0},{8,12},{12,8},{16,20},{20,16},{24,28},{28,24},{1,5},{5... | collective-permute-start | bytes 393224 | tf_op jit(solution)/shard_map/ppermute | solution.py:29
  179.8 26.2 %collective-permute-start.39 = (bf16[128,512]{1,0:T(8,128)(2,1)S(1)}, bf16[128,512]{1,0:T(8,128)(2,1)S(1)}, u32[]{:S(2)}, u32[]{:S(2)}) collective-permute-start(bf16[128,512]{1,0:T(8,128)(2,1)S(1)} %fusion.14), channel_id=1, source_target_pairs={{0,8},{4,12},{8,16},{12,20},{16,24},{20,28},{1,9},{5,13},{9,17},{1... | collective-permute-start | bytes 393224 | tf_op jit(solution)/shard_map/ppermute | solution.py:318
  183.2 24.1 %collective-permute-start.40 = (bf16[128,512]{1,0:T(8,128)(2,1)S(1)}, bf16[128,512]{1,0:T(8,128)(2,1)S(1)}, u32[]{:S(2)}, u32[]{:S(2)}) collective-permute-start(bf16[128,512]{1,0:T(8,128)(2,1)S(1)} %fusion.14), channel_id=1, source_target_pairs={{0,16},{4,20},{8,24},{12,28},{1,17},{5,21},{9,25},{13,29},{2,18},{... | collective-permute-start | bytes 393224 | tf_op jit(solution)/shard_map/ppermute | solution.py:318
  188.0 20.9 %collective-permute-start.41 = (bf16[128,512]{1,0:T(8,128)(2,1)S(1)}, bf16[128,512]{1,0:T(8,128)(2,1)}, u32[]{:S(2)}, u32[]{:S(2)}) collective-permute-start(bf16[128,512]{1,0:T(8,128)(2,1)S(1)} %fusion.14), channel_id=1, source_target_pairs={{0,24},{4,28},{1,25},{5,29},{2,26},{6,30},{3,27},{7,31}} | collective-permute-start | bytes 393224 | tf_op jit(solution)/shard_map/ppermute | solution.py:318
  204.7 7.9 %collective-permute-start.44 = (bf16[128,512]{1,0:T(8,128)(2,1)S(1)}, bf16[128,512]{1,0:T(8,128)(2,1)}, u32[]{:S(2)}, u32[]{:S(2)}) collective-permute-start(bf16[128,512]{1,0:T(8,128)(2,1)S(1)} %fusion.16), channel_id=1, source_target_pairs={{8,0},{12,4},{16,8},{20,12},{24,16},{28,20},{9,1},{13,5},{17,9},{2... | collective-permute-start | bytes 393224 | tf_op jit(solution)/shard_map/ppermute | solution.py:318
  206.0 14.9 %collective-permute-start.45 = (bf16[128,512]{1,0:T(8,128)(2,1)S(1)}, bf16[128,512]{1,0:T(8,128)(2,1)}, u32[]{:S(2)}, u32[]{:S(2)}) collective-permute-start(bf16[128,512]{1,0:T(8,128)(2,1)S(1)} %fusion.16), channel_id=1, source_target_pairs={{16,0},{20,4},{24,8},{28,12},{17,1},{21,5},{25,9},{29,13},{18,2},{... | collective-permute-start | bytes 393224 | tf_op jit(solution)/shard_map/ppermute | solution.py:318
  207.4 13.6 %collective-permute-start.46 = (bf16[128,512]{1,0:T(8,128)(2,1)S(1)}, bf16[128,512]{1,0:T(8,128)(2,1)}, u32[]{:S(2)}, u32[]{:S(2)}) collective-permute-start(bf16[128,512]{1,0:T(8,128)(2,1)S(1)} %fusion.16), channel_id=1, source_target_pairs={{24,0},{28,4},{25,1},{29,5},{26,2},{30,6},{27,3},{31,7}} | collective-permute-start | bytes 393224 | tf_op jit(solution)/shard_map/ppermute | solution.py:318
  208.9 22.7 %copy-start.9 = (bf16[8,256,128]{2,1,0:T(8,128)(2,1)}, bf16[8,256,128]{2,1,0:T(8,128)(2,1)S(1)}, u32[]{:S(2)}) copy-start(bf16[8,256,128]{2,1,0:T(8,128)(2,1)S(1)} %all-to-all-done.mine_ref) | copy-start | bytes 1572868
  208.9 29.2 %collective-permute-start.33 = (bf16[8,256,128]{2,1,0:T(8,128)(2,1)S(1)}, bf16[8,256,128]{2,1,0:T(8,128)(2,1)}, u32[]{:S(2)}, u32[]{:S(2)}) collective-permute-start(bf16[8,256,128]{2,1,0:T(8,128)(2,1)S(1)} %all-to-all-done.mine_ref), channel_id=1, source_target_pairs={{0,1},{1,0},{2,3},{3,2},{4,5},{5,4},{6,7},{7,6},{8,9},{9,8},{10,11... | collective-permute-start | bytes 1572872 | tf_op jit(solution)/shard_map/ppermute | solution.py:29
  212.6 19.0 %collective-permute-start.42 = (bf16[128,512]{1,0:T(8,128)(2,1)}, bf16[128,512]{1,0:T(8,128)(2,1)S(1)}, u32[]{:S(2)}, u32[]{:S(2)}) collective-permute-start(bf16[128,512]{1,0:T(8,128)(2,1)} %get-tuple-element.51), channel_id=1, source_target_pairs={{0,4},{4,0},{8,12},{12,8},{16,20},{20,16},{24,28},{28,24},{1,5},{5... | collective-permute-start | bytes 393224 | tf_op jit(solution)/shard_map/ppermute | solution.py:29
  222.8 12.1 %collective-permute-start.47 = (bf16[128,512]{1,0:T(8,128)(2,1)S(1)}, bf16[128,512]{1,0:T(8,128)(2,1)S(1)}, u32[]{:S(2)}, u32[]{:S(2)}) collective-permute-start(bf16[128,512]{1,0:T(8,128)(2,1)S(1)} %get-tuple-element.49), channel_id=1, source_target_pairs={{0,4},{4,0},{8,12},{12,8},{16,20},{20,16},{24,28},{28,24},{1,5},{5... | collective-permute-start | bytes 393224 | tf_op jit(solution)/shard_map/ppermute | solution.py:29
  (26 other events, 89.3 us)
where the time goes:
time: 242 us
  waiting for transfers between devices  92.5 us (38%)
  starting transfers between devices  83.3 us (34%)
  Pallas kernels  41.8 us (17%)
  other arithmetic  11.4 us (5%)
  local copies, waits for them, and re-layouts  6.78 us (3%)
  matrix products  4.1 us (2%)
    ppermute x42, waiting for transfers between devices, swap(): lax.ppermute(x, axis, [(i, i ^ bits) for i in range(lax.axis_size(axis))])  82.5 us
    ppermute x42, starting transfers between devices, swap(): lax.ppermute(x, axis, [(i, i ^ bits) for i in range(lax.axis_size(axis))])  53.2 us
    pallas_call x7, Pallas kernels, call(): pl.pallas_call(body, in_specs=[smem] * len(scalars) + [vmem] * len(args),...  19.8 us
    all_to_all x1, starting transfers between devices, transpose_blocks(): return lax.all_to_all(x, 'sp', split_axis=0, concat_axis=0, tiled=True)  15.9 us
    ppermute x6, starting transfers between devices, carry_outer(): lax.ppermute(total, 'sp', [(i, i + sign * d) for i in range(count) if 0 <...  14.1 us
    ppermute x6, waiting for transfers between devices, carry_outer(): lax.ppermute(total, 'sp', [(i, i + sign * d) for i in range(count) if 0 <...  10 us
    pallas_call x1, Pallas kernels, grad_call(): pl.pallas_call(grad_body, grid_spec=pltpu.PrefetchScalarGridSpec(num_scal...  8.19 us
    pallas_call x1, Pallas kernels, expert_call(): pl.pallas_call(expert_body, grid_spec=pltpu.PrefetchScalarGridSpec(num_sc...  7.57 us
  transfers between devices with their start and end apart: 49, of which 13 were waited for; matrix products, arithmetic and copies ran while one was open for 7% of the time, Pallas kernels for 13%

commit v1 on v0

--- a/solution.py
+++ b/solution.py
@@ -82,7 +82,7 @@
     return pl.CostEstimate(flops=int(count), bytes_accessed=0, transcendentals=0)
 
 
-def call(body, outs, *args, scalars=(), work=0):
+def call(body, outs, *args, scalars=(), work=0, scratch=()):
     vmem = pl.BlockSpec(memory_space=pltpu.VMEM)
     smem = pl.BlockSpec(memory_space=pltpu.SMEM)
     return pl.pallas_call(
@@ -90,6 +90,7 @@
         in_specs=[smem] * len(scalars) + [vmem] * len(args),
         out_specs=[vmem] * len(outs),
         out_shape=[jax.ShapeDtypeStruct(shape, kind) for shape, kind in outs],
+        scratch_shapes=[pltpu.VMEM(shape, kind) for shape, kind in scratch],
         cost_estimate=flops(work),
     )(*scalars, *args)
 
@@ -102,25 +103,28 @@
     layer_ref[...] = (cot_ref[...].astype(F32) + total).astype(BF16)
 
 
-def mix_body(place_ref, *refs):
-    pieces, (weight_ref, query_ref, send_ref, mixed_ref, state_ref) = refs[:-5], refs[-5:]
-    place = place_ref[0]
+def mix_body(ids_ref, *refs):
+    pieces, (weight_ref, query_ref) = refs[:-6], refs[-6:-4]
+    send_ref, mixed_ref, mine_ref, theirs_ref = refs[-4:]
+    place = ids_ref[0]
     cols = pieces[0].shape[1]
-    half = send_ref.shape[2]
-    count = send_ref.shape[0] // len(pieces)
+    count, rows, width = send_ref.shape
+    count //= len(pieces)
     total = None
     for k, piece in enumerate(pieces):
         block = place ^ k
-        x = piece[...]
+        x = piece[pl.ds(place * rows, rows), :]
         for q in range(count):
-            low = x[:, 2 * q * half : (2 * q + 1) * half]
-            high = x[:, (2 * q + 1) * half : (2 * q + 2) * half]
-            send_ref[block * count + q] = jnp.where(place % 2 == 0, low, high)
-        part = dot(x, weight_ref[pl.ds(block * cols, cols), :])
+            send_ref[block * count + q] = x[:, q * width : (q + 1) * width]
+        part = dot(piece[...], weight_ref[pl.ds(block * cols, cols), :])
         total = part if total is None else total + part
     mixed = total.astype(BF16)
     mixed_ref[...] = mixed
-    state_ref[...] = dot(query_ref[...], mixed, ROWS).astype(BF16)
+    state = dot(query_ref[...], mixed, ROWS).astype(BF16)
+    half = mine_ref.shape[0]
+    low = ids_ref[1] % 2 == 0
+    mine_ref[...] = jnp.where(low, state[:half], state[half:])
+    theirs_ref[...] = jnp.where(low, state[half:], state[:half])
 
 
 def decays(rates_ref, count):
@@ -153,11 +157,13 @@
     value_near_ref[...] = dot(near_qk, mixed, ROWS)
 
 
-def last_body(ids_ref, rates_ref, own_ref, got_ref, key_ref, value_ref, kn_ref, vn_ref, kg_ref, vg_ref):
+def last_body(ids_ref, rates_ref, own_ref, got_ref, key_ref, value_ref, kn_ref, vn_ref, *refs):
+    kg_ref, vg_ref = refs[-4:-2]
     later = paired(ids_ref[1] % 2 == 0, own_ref, got_ref)
     _, trailing = decays(rates_ref, key_ref.shape[0])
     kg_ref[...] = kn_ref[...] + trailing * dot(value_ref[...], later, COLS)
     vg_ref[...] = vn_ref[...] + trailing * dot(key_ref[...], later)
+    proj_body(ids_ref, *refs[:-4], *refs[-2:])
 
 
 def pre_body(place_ref, *refs):
@@ -281,16 +287,19 @@
     )(place, *ups, down, down, partial, gate_pre, up_pre, *[gate] * pieces, *[up] * pieces)
 
 
-def proj_body(place_ref, mine_ref, theirs_ref, even_ref, odd_ref, out_ref):
-    place = place_ref[1]
-    core = place_ref[0] % 2
-    for rows_ref, slot in ((mine_ref, core), (theirs_ref, 1 - core)):
-        total = None
-        for k in range(even_ref.shape[0]):
-            for kept_ref, low in ((even_ref, 0), (odd_ref, 1)):
-                part = dot(rows_ref[place ^ (2 * k + low)], kept_ref[k], ROWS)
-                total = part if total is None else total + part
-        out_ref[slot] = total
+def proj_body(ids_ref, *refs):
+    pieces, (even_ref, odd_ref, out_ref, rows_ref) = refs[:-4], refs[-4:]
+    count, rows, _ = pieces[0].shape
+    for k, piece in enumerate(pieces):
+        start = pl.multiple_of((ids_ref[0] ^ k) * rows, rows)
+        for source in range(count):
+            rows_ref[source, pl.ds(start, rows), :] = piece[source]
+    total = None
+    for k in range(count):
+        kept_ref = odd_ref if k % 2 else even_ref
+        part = dot(rows_ref[ids_ref[1] ^ k], kept_ref[k // 2], ROWS)
+        total = part if total is None else total + part
+    out_ref[...] = total
 
 
 def dot(a, b, dims=None):
@@ -302,10 +311,9 @@
 def carry_pair(state, span, reverse):
     low = lax.axis_index("sp") % 2
     first = (low == 1) if reverse else (low == 0)
-    half = state.shape[0] // 2
-    mine = lax.dynamic_slice_in_dim(state, low * half, half, 0)
-    theirs = swap(lax.dynamic_slice_in_dim(state, (1 - low) * half, half, 0), "sp", 1)
-    mine, theirs = mine.astype(F32), theirs.astype(F32)
+    mine, sent = state
+    theirs = swap(sent, "sp", 1).astype(F32)
+    mine = mine.astype(F32)
     early = jnp.where(first, mine, theirs)
     late = jnp.where(first, theirs, mine)
     return early, (late + jnp.exp(span) * early).astype(BF16)
@@ -390,7 +398,13 @@
     key_decayed = (key_rows.astype(F32) * suffix_decay).astype(BF16)
     query_decayed = (queries.astype(F32) * prefix_decay).astype(BF16)
     prior_state = dot(key_decayed, value_rows, ROWS).astype(BF16)
-    prior_early, prior_total = carry_pair(prior_state, span, False)
+    state_rows = prior_state.shape[0] // 2
+    low = sp_place % 2
+    halves = [
+        lax.dynamic_slice_in_dim(prior_state, place * state_rows, state_rows, 0)
+        for place in (low, 1 - low)
+    ]
+    prior_early, prior_total = carry_pair(halves, span, False)
     ins = gather_tp(got_in)
     ups = gather_tp(got_up)
     kept = [retained] + [swap(retained, "sp", k) for k in range(2, sp_count, 2)]
@@ -424,14 +438,15 @@
     )
 
     layers = gather_tp(layer_cols)
-    half = width // sp_count // 2
     values = value_rows.shape[1]
-    layer_send, mixed_grad, state = call(
+    part = width // sp_count
+    layer_send, mixed_grad, *state = call(
         mix_body,
         (
-            ((sp_count, tokens, half), BF16),
+            ((sp_count, tokens // tp_count, part), BF16),
             ((tokens, values), BF16),
-            ((queries.shape[1], values), BF16),
+            ((queries.shape[1] // 2, values), BF16),
+            ((queries.shape[1] // 2, values), BF16),
         ),
         *layers,
         out_weight,
@@ -445,7 +460,7 @@
     mine = transpose_blocks(layer_send)
     later_own, later_sent = carry_inner(later_early, later_outer, span, True)
     later_got = swap(later_sent, "sp", 1)
-    theirs = swap(mine, "tp", 1)
+    layer_rows = gather_tp(mine)
     query_gradient, key_near, value_near = call(
         near_body,
         ((queries.shape, F32), (queries.shape, F32), (value_rows.shape, F32)),
@@ -458,29 +473,22 @@
         scalars=(ids, rates),
         work=10 * tokens * tokens * values,
     )
-    key_gradient, value_gradient = call(
+    key_gradient, value_gradient, proj_grad = call(
         last_body,
-        ((key_near.shape, F32), (value_near.shape, F32)),
+        ((key_near.shape, F32), (value_near.shape, F32), ((part, retained.shape[1]), F32)),
         later_own,
         later_got,
         key_rows,
         value_rows,
         key_near,
         value_near,
-        scalars=(ids, rates),
-        work=4 * tokens * values * queries.shape[1],
-    )
-    (proj_grad,) = call(
-        proj_body,
-        (((2, half, retained.shape[1]), F32),),
-        mine,
-        theirs,
+        *layer_rows,
         even,
         odd,
-        scalars=(ids,),
-        work=2 * sp_count * tokens * 2 * half * retained.shape[1],
-    )
-    proj_grad = proj_grad.reshape(2 * half, retained.shape[1])
+        scalars=(ids, rates),
+        work=2 * sp_count * tokens * part * retained.shape[1],
+        scratch=(((sp_count, tokens, part), BF16),),
+    )
     return (
         gate_grad[None],
         up_grad[None],

time: 242 us -> 241 us (level)
  other arithmetic: 11.4 us -> 14.8 us
  waiting for transfers between devices: 92.5 us -> 89.9 us
    convert_element_type x2, other arithmetic: 0.14 us -> 2.58 us  [carry_pair(): return (early, (late + jnp.exp(span) * early).astype(BF16))]
    pallas_call x7 -> x6, Pallas kernels: 19.8 us -> 17.8 us  [call(): pl.pallas_call(body, in_specs=[smem] * len(scalars) + [vmem] * len(args),...]
    ppermute x42 -> x44, starting transfers between devices: 53.2 us -> 51.3 us  [swap(): lax.ppermute(x, axis, [(i, i ^ bits) for i in range(lax.axis_size(axis))])]
    ppermute x42 -> x44, waiting for transfers between devices: 82.5 us -> 81.6 us  [swap(): lax.ppermute(x, axis, [(i, i ^ bits) for i in range(lax.axis_size(axis))])]
  transfers between devices with their start and end apart: 49 -> 51, of which waited for: 13 -> 12; matrix products, arithmetic and copies ran while one was open for 7% -> 8% of each run, Pallas kernels for 13% -> 12%
where the time goes in v1:
time: 241 us; the launch traced here: 240 us
  waiting for transfers between devices  89.9 us (37%)
  starting transfers between devices  82.6 us (34%)
  Pallas kernels  39.8 us (17%)
  other arithmetic  14.8 us (6%)
  local copies, waits for them, and re-layouts  7.05 us (3%)
  matrix products  4.1 us (2%)
    ppermute x44, waiting for transfers between devices, swap(): lax.ppermute(x, axis, [(i, i ^ bits) for i in range(lax.axis_size(axis))])  81.6 us
    ppermute x44, starting transfers between devices, swap(): lax.ppermute(x, axis, [(i, i ^ bits) for i in range(lax.axis_size(axis))])  51.3 us
    pallas_call x6, Pallas kernels, call(): pl.pallas_call(body, in_specs=[smem] * len(scalars) + [vmem] * len(args),...  17.8 us
    all_to_all x1, starting transfers between devices, transpose_blocks(): return lax.all_to_all(x, 'sp', split_axis=0, concat_axis=0, tiled=True)  16.5 us
    ppermute x6, starting transfers between devices, carry_outer(): lax.ppermute(total, 'sp', [(i, i + sign * d) for i in range(count) if 0 <...  14.8 us
    ppermute x6, waiting for transfers between devices, carry_outer(): lax.ppermute(total, 'sp', [(i, i + sign * d) for i in range(count) if 0 <...  8.33 us
    pallas_call x1, Pallas kernels, grad_call(): pl.pallas_call(grad_body, grid_spec=pltpu.PrefetchScalarGridSpec(num_scal...  8.18 us
    pallas_call x1, Pallas kernels, expert_call(): pl.pallas_call(expert_body, grid_spec=pltpu.PrefetchScalarGridSpec(num_sc...  7.56 us
  transfers between devices with their start and end apart: 51, of which 12 were waited for; matrix products, arithmetic and copies ran while one was open for 8% of the time, Pallas kernels for 12%

profile of v1, /device:TPU:0, one launch (start us, length us, event | category | flops | bytes accessed | tf_op | source)
XLA Modules:
  0.0 239.8 jit_solution(7878395541185821437)
XLA Ops:
  0.7 0.8 copy.19
  2.3 3.1 %collective-permute-start = (bf16[96,512]{1,0:T(8,128)(2,1)S(1)}, bf16[96,512]{1,0:T(8,128)(2,1)S(1)}, u32[]{:S(2)}, u32[]{:S(2)}) collective-permute-start(bf16[96,512]{1,0:T(8,128)(2,1)S(1)} %get-tuple-element.75), channel_id=1, source_target_pairs={{0,4},{4,0},{8,12},{12,8},{16,20},{20,16},{24,28},{28,24},{1,5},{5... | collective-permute-start | bytes 294920 | tf_op jit(solution)/shard_map/ppermute | solution.py:29
  5.4 1.6 collective-permute-start.1
  7.0 3.0 %collective-permute-start.3 = (bf16[96,512]{1,0:T(8,128)(2,1)S(1)}, bf16[96,512]{1,0:T(8,128)(2,1)S(1)}, u32[]{:S(2)}, u32[]{:S(2)}) collective-permute-start(bf16[96,512]{1,0:T(8,128)(2,1)S(1)} %get-tuple-element.72), channel_id=1, source_target_pairs={{0,16},{4,20},{8,24},{12,28},{16,0},{20,4},{24,8},{28,12},{1,17},{... | collective-permute-start | bytes 294920 | tf_op jit(solution)/shard_map/ppermute | solution.py:29
  10.0 1.3 collective-permute-start.4
  11.5 1.1 fusion.6
  13.4 3.7 %collective-permute-start.5 = (bf16[96,512]{1,0:T(8,128)(2,1)S(1)}, bf16[96,512]{1,0:T(8,128)(2,1)S(1)}, u32[]{:S(2)}, u32[]{:S(2)}) collective-permute-start(bf16[96,512]{1,0:T(8,128)(2,1)S(1)} %get-tuple-element.70), channel_id=1, source_target_pairs={{0,24},{4,28},{8,16},{12,20},{16,8},{20,12},{24,0},{28,4},{1,25},{... | collective-permute-start | bytes 294920 | tf_op jit(solution)/shard_map/ppermute | solution.py:29
  17.1 0.8 fusion.31
  17.9 1.7 collective-permute-start.10
  19.6 1.0 collective-permute-start.11
  20.5 4.7 %collective-permute-done.4.refs_4_ = bf16[96,512]{1,0:T(8,128)(2,1)S(1)} collective-permute-done((bf16[96,512]{1,0:T(8,128)(2,1)S(1)}, bf16[96,512]{1,0:T(8,128)(2,1)S(1)}, u32[]{:S(2)}, u32[]{:S(2)}) %collective-permute-start.4) | collective-permute-done | bytes 98336 | tf_op jit(solution)/shard_map/ppermute | solution.py:29
  25.9 2.3 shard_map.171
  28.2 1.5 collective-permute-start.8
  29.7 5.1 %collective-permute-start.13 = (bf16[96,512]{1,0:T(8,128)(2,1)}, bf16[96,512]{1,0:T(8,128)(2,1)S(1)}, u32[]{:S(2)}, u32[]{:S(2)}) collective-permute-start(bf16[96,512]{1,0:T(8,128)(2,1)} %get-tuple-element.65), channel_id=1, source_target_pairs={{0,16},{4,20},{8,24},{12,28},{16,0},{20,4},{24,8},{28,12},{1,17},{... | collective-permute-start | bytes 294920 | tf_op jit(solution)/shard_map/ppermute | solution.py:29
  34.8 0.8 collective-permute-start.14
  35.6 1.0 collective-permute-start.15
  36.6 3.0 %collective-permute-start.16 = (bf16[96,512]{1,0:T(8,128)(2,1)}, bf16[96,512]{1,0:T(8,128)(2,1)}, u32[]{:S(2)}, u32[]{:S(2)}) collective-permute-start(bf16[96,512]{1,0:T(8,128)(2,1)} %get-tuple-element.62), channel_id=1, source_target_pairs={{0,28},{4,24},{8,20},{12,16},{16,12},{20,8},{24,4},{28,0},{1,29},{... | collective-permute-start | bytes 294920 | tf_op jit(solution)/shard_map/ppermute | solution.py:29
  39.6 6.8 %collective-permute-done.13.refs_3_ = bf16[96,512]{1,0:T(8,128)(2,1)S(1)} collective-permute-done((bf16[96,512]{1,0:T(8,128)(2,1)}, bf16[96,512]{1,0:T(8,128)(2,1)S(1)}, u32[]{:S(2)}, u32[]{:S(2)}) %collective-permute-start.13) | collective-permute-done | bytes 98336 | tf_op jit(solution)/shard_map/ppermute | solution.py:29
  46.4 1.8 collective-permute-done.14.refs_4_
  48.8 2.3 shard_map.172
  52.3 17.1 %collective-permute-done.18.refs_0_.refs_6_ = bf16[768,512]{1,0:T(8,128)(2,1)} collective-permute-done((bf16[768,512]{1,0:T(8,128)(2,1)}, bf16[768,512]{1,0:T(8,128)(2,1)}, u32[]{:S(2)}, u32[]{:S(2)}) %collective-permute-start.18) | collective-permute-done | bytes 786464 | tf_op jit(solution)/shard_map/ppermute | solution.py:29
  70.0 1.5 fusion.17
  71.5 1.3 convolution_add_fusion.refs_4_
  72.8 6.2 %shard_map.173 = (f32[768,256]{1,0:T(8,128)}, f32[768,256]{1,0:T(8,128)}) custom-call(s32[2]{0:T(128)} %pad_add_fusion.place_ref.ids_ref, bf16[768,512]{1,0:T(8,128)(2,1)} %bitcast.53, bf16[768,512]{1,0:T(8,128)(2,1)} %collective-permute-done.7.refs_1_, bf16[768,512]{1,0:T(8,128)(2,1)} %collective-permute-done.8.refs_2_, ...), custom_call_target="tpu_custom_call" | custom-call | flops 1610612736 | tf_op jit(solution)/shard_map/pallas_call | solution.py:185
  79.0 7.6 %shard_map.174 = (bf16[768,256]{1,0:T(8,128)(2,1)}, bf16[768,256]{1,0:T(8,128)(2,1)}, bf16[768,256]{1,0:T(8,128)(2,1)}, bf16[768,512]{1,0:T(8,128)(2,1)}, bf16[7...) custom-call(s32[2]{0:T(128)} %pad_add_fusion.place_ref.ids_ref, ...), custom_call_target="tpu_custom_call" | custom-call | flops 2415919104 | tf_op jit(solution)/shard_map/pallas_call | solution.py:272
  87.2 2.0 collective-permute-done.21
  89.3 1.3 add_convert_fusion.1
  91.2 19.3 %collective-permute-done.22 = bf16[768,512]{1,0:T(8,128)(2,1)S(1)} collective-permute-done((bf16[768,512]{1,0:T(8,128)(2,1)S(1)}, bf16[768,512]{1,0:T(8,128)(2,1)S(1)}, u32[]{:S(2)}, u32[]{:S(2)}) %collective-permute-start.22) | collective-permute-done | bytes 786464 | tf_op jit(solution)/shard_map/ppermute | solution.py:29
  110.9 0.7 fusion.30
  111.6 1.4 collective-permute-start.23
  113.0 4.3 %collective-permute-start.24 = (bf16[96,512]{1,0:T(8,128)(2,1)S(1)}, bf16[96,512]{1,0:T(8,128)(2,1)S(1)}, u32[]{:S(2)}, u32[]{:S(2)}) collective-permute-start(bf16[96,512]{1,0:T(8,128)(2,1)S(1)} %get-tuple-element.60), channel_id=1, source_target_pairs={{0,8},{4,12},{8,0},{12,4},{16,24},{20,28},{24,16},{28,20},{1,9},{5... | collective-permute-start | bytes 294920 | tf_op jit(solution)/shard_map/ppermute | solution.py:29
  117.3 1.0 fusion.11.pick_ref
  118.5 2.9 %collective-permute-start.26 = (bf16[96,512]{1,0:T(8,128)(2,1)S(1)}, bf16[96,512]{1,0:T(8,128)(2,1)}, u32[]{:S(2)}, u32[]{:S(2)}) collective-permute-start(bf16[96,512]{1,0:T(8,128)(2,1)S(1)} %get-tuple-element.58), channel_id=1, source_target_pairs={{0,16},{4,20},{8,24},{12,28},{16,0},{20,4},{24,8},{28,12},{1,17},{... | collective-permute-start | bytes 294920 | tf_op jit(solution)/shard_map/ppermute | solution.py:29
  121.3 1.0 collective-permute-start.27
  122.3 2.4 collective-permute-start.28
  124.7 1.5 collective-permute-start.29
  126.4 4.7 %collective-permute-done.26.refs_3_ = bf16[96,512]{1,0:T(8,128)(2,1)} collective-permute-done((bf16[96,512]{1,0:T(8,128)(2,1)S(1)}, bf16[96,512]{1,0:T(8,128)(2,1)}, u32[]{:S(2)}, u32[]{:S(2)}) %collective-permute-start.26) | collective-permute-done | bytes 98336 | tf_op jit(solution)/shard_map/ppermute | solution.py:29
  131.2 5.1 %collective-permute-done.27.refs_4_ = bf16[96,512]{1,0:T(8,128)(2,1)} collective-permute-done((bf16[96,512]{1,0:T(8,128)(2,1)S(1)}, bf16[96,512]{1,0:T(8,128)(2,1)}, u32[]{:S(2)}, u32[]{:S(2)}) %collective-permute-start.27) | collective-permute-done | bytes 98336 | tf_op jit(solution)/shard_map/ppermute | solution.py:29
  136.2 2.6 %collective-permute-start.48 = (bf16[256,512]{1,0:T(8,128)(2,1)S(1)}, bf16[256,512]{1,0:T(8,128)(2,1)S(1)}, u32[]{:S(2)}, u32[]{:S(2)}) collective-permute-start(bf16[256,512]{1,0:T(8,128)(2,1)S(1)} %copy-done.15), channel_id=1, source_target_pairs={{0,24},{4,28},{8,16},{12,20},{16,8},{20,12},{24,0},{28,4},{1,25},{... | collective-permute-start | bytes 786440 | tf_op jit(solution)/shard_map/ppermute | solution.py:29
  138.8 3.0 %shard_map.176.refs_0_ = bf16[256,512]{1,0:T(8,128)(2,1)} custom-call(bf16[8,96,256]{2,1,0:T(8,128)(2,1)} %fusion.11.pick_ref, bf16[8,96,512]{2,1,0:T(8,128)(2,1)} %bitcast.51, bf16[96,512]{1,0:T(8,128)(2,1)} %copy-done.23, bf16[96,512]{1,0:T(8,128)(2,1)} %copy-done.24, bf16[96,512]{1,0:T(8,128)(2,1)} %collective-permute-done.25.refs_2_, ...), custom_call_target="tpu_custom_call" | custom-call | flops 201326592 | tf_op jit(solution)/shard_map/pallas_call | solution.py:88
  143.0 5.3 %collective-permute-done.31.refs_2_ = bf16[256,512]{1,0:T(8,128)(2,1)S(1)} collective-permute-done((bf16[256,512]{1,0:T(8,128)(2,1)}, bf16[256,512]{1,0:T(8,128)(2,1)S(1)}, u32[]{:S(2)}, u32[]{:S(2)}) %collective-permute-start.31) | collective-permute-done | bytes 262176 | tf_op jit(solution)/shard_map/ppermute | solution.py:29
  148.4 1.8 multiply_convert_fusion.1.refs_5_
  151.5 3.6 %shard_map.177 = (bf16[8,64,256]{2,1,0:T(8,128)(2,1)}, bf16[256,512]{1,0:T(8,128)(2,1)}, bf16[128,512]{1,0:T(8,128)(2,1)}, bf16[128,512]{1,0:T(8,128)(2,1)}) custom-call(s32[2]{0:T(128)} %pad_add_fusion.place_ref.ids_ref, bf16[256,512]{1,0:T(8,128)(2,1)} %shard_map.176.refs_0_, bf16[256,512]{1,0:T(8,128)(2,1)} %copy-done.21, bf16[256,512]{1,0:T(8,128)(2,1)} %copy-done.20, ...), custom_call_target="tpu_custom_call" | custom-call | flops 536870912 | tf_op jit(solution)/shard_map/pallas_call | solution.py:88
  155.1 16.5 %all-to-all-start = ((bf16[8,64,256]{2,1,0:T(8,128)(2,1)}), bf16[8,64,256]{2,1,0:T(8,128)(2,1)}, u32[]{:S(2)}, u32[]{:S(2)}) async-start(bf16[8,64,256]{2,1,0:T(8,128)(2,1)} %get-tuple-element.46), calls=%async_computation | async-start | bytes 524288 | tf_op jit(solution)/shard_map/all_to_all | solution.py:43
  173.0 1.2 pad_maximum_fusion.refs_4_
  174.3 2.1 collective-permute-start.49
  176.5 1.6 fusion.16
  178.1 4.5 %collective-permute-start.39 = (bf16[128,512]{1,0:T(8,128)(2,1)}, bf16[128,512]{1,0:T(8,128)(2,1)}, u32[]{:S(2)}, u32[]{:S(2)}) collective-permute-start(bf16[128,512]{1,0:T(8,128)(2,1)} %fusion.16), channel_id=1, source_target_pairs={{0,8},{4,12},{8,16},{12,20},{16,24},{20,28},{1,9},{5,13},{9,17},{1... | collective-permute-start | bytes 393224 | tf_op jit(solution)/shard_map/ppermute | solution.py:326
  182.6 4.3 %collective-permute-start.40 = (bf16[128,512]{1,0:T(8,128)(2,1)}, bf16[128,512]{1,0:T(8,128)(2,1)}, u32[]{:S(2)}, u32[]{:S(2)}) collective-permute-start(bf16[128,512]{1,0:T(8,128)(2,1)} %fusion.16), channel_id=1, source_target_pairs={{0,16},{4,20},{8,24},{12,28},{1,17},{5,21},{9,25},{13,29},{2,18},{... | collective-permute-start | bytes 393224 | tf_op jit(solution)/shard_map/ppermute | solution.py:326
  186.9 2.0 collective-permute-start.41
  188.8 14.7 %collective-permute-done.33 = bf16[128,512]{1,0:T(8,128)(2,1)} collective-permute-done((bf16[128,512]{1,0:T(8,128)(2,1)S(1)}, bf16[128,512]{1,0:T(8,128)(2,1)}, u32[]{:S(2)}, u32[]{:S(2)}) %collective-permute-start.33) | collective-permute-done | bytes 131104 | tf_op jit(solution)/shard_map/ppermute | solution.py:29
  204.0 1.0 fusion.14
  205.0 1.3 collective-permute-start.34
  206.3 1.3 collective-permute-start.35
  207.6 1.5 collective-permute-start.36
  209.1 2.0 select_convert_fusion
  211.1 1.9 collective-permute-done.34
  213.0 1.4 collective-permute-start.42
  214.4 6.4 %collective-permute-done.35 = bf16[128,512]{1,0:T(8,128)(2,1)S(1)} collective-permute-done((bf16[128,512]{1,0:T(8,128)(2,1)S(1)}, bf16[128,512]{1,0:T(8,128)(2,1)S(1)}, u32[]{:S(2)}, u32[]{:S(2)}) %collective-permute-start.35) | collective-permute-done | bytes 131104 | tf_op jit(solution)/shard_map/ppermute | solution.py:326
  221.3 1.8 select_convert_fusion.2
  223.7 8.2 %shard_map.175 = (f32[4,512,256]{2,1,0:T(8,128)}, f32[4,512,256]{2,1,0:T(8,128)}, f32[256,2048]{1,0:T(8,128)}) custom-call(s32[2]{0:T(128)} %pad_add_fusion.place_ref.ids_ref, bf16[768,512]{1,0:T(8,128)(2,1)} %bitcast.54, bf16[768,512]{1,0:T(8,128)(2,1)} %collective-permute-done.7.refs_1_, bf16[768,512]{1,0:T(8,128)(2,1)} %collective-permute-done.8.refs_2_, ...), custom_call_target="tpu_custom_call" | custom-call | flops 2415919104 | tf_op jit(solution)/shard_map/pallas_call | solution.py:224
  231.9 2.7 %shard_map.178 = (f32[256,256]{1,0:T(8,128)}, f32[256,256]{1,0:T(8,128)}, f32[256,512]{1,0:T(8,128)}) custom-call(s32[2]{0:T(128)} %pad_add_fusion.place_ref.ids_ref, f32[2]{0:T(128)} %pad_maximum_fusion.1.rates_ref, bf16[256,512]{1,0:T(8,128)(2,1)} %get-tuple-element.43.mixed_ref, bf16[256,256]{1,0:T(8,128)(2,1)} %query_ref.1, bf16[256,256]{1,0:T(8,128)(2,1)} %key_ref.3, ...), custom_call_target="tpu_custom_call" | custom-call | flops 335544320 | tf_op jit(solution)/shard_map/pallas_call | solution.py:88
  234.7 0.9 copy-done.9
  235.8 4.0 %shard_map.179 = (f32[256,256]{1,0:T(8,128)}, f32[256,512]{1,0:T(8,128)}, f32[256,512]{1,0:T(8,128)}) custom-call(s32[2]{0:T(128)} %pad_add_fusion.place_ref.ids_ref, f32[2]{0:T(128)} %pad_maximum_fusion.1.rates_ref, bf16[128,512]{1,0:T(8,128)(2,1)} %get-tuple-element.77.own_ref, bf16[128,512]{1,0:T(8,128)(2,1)} %copy-done.22, bf16[256,256]{1,0:T(8,128)(2,1)} %key_ref.3, ...), custom_call_target="tpu_custom_call" | custom-call | flops 536870912 | tf_op jit(solution)/shard_map/pallas_call | solution.py:88
  (158 shorter events, 12.7 us)
Async XLA Ops:
  2.3 11.0 %collective-permute-start = (bf16[96,512]{1,0:T(8,128)(2,1)S(1)}, bf16[96,512]{1,0:T(8,128)(2,1)S(1)}, u32[]{:S(2)}, u32[]{:S(2)}) collective-permute-start(bf16[96,512]{1,0:T(8,128)(2,1)S(1)} %get-tuple-element.75), channel_id=1, source_target_pairs={{0,4},{4,0},{8,12},{12,8},{16,20},{20,16},{24,28},{28,24},{1,5},{5... | collective-permute-start | bytes 294920 | tf_op jit(solution)/shard_map/ppermute | solution.py:29
  5.4 11.6 %collective-permute-start.1 = (bf16[96,512]{1,0:T(8,128)(2,1)S(1)}, bf16[96,512]{1,0:T(8,128)(2,1)S(1)}, u32[]{:S(2)}, u32[]{:S(2)}) collective-permute-start(bf16[96,512]{1,0:T(8,128)(2,1)S(1)} %get-tuple-element.74), channel_id=1, source_target_pairs={{0,8},{4,12},{8,0},{12,4},{16,24},{20,28},{24,16},{28,20},{1,9},{5... | collective-permute-start | bytes 294920 | tf_op jit(solution)/shard_map/ppermute | solution.py:29
  7.0 10.9 %collective-permute-start.2 = (bf16[96,512]{1,0:T(8,128)(2,1)S(1)}, bf16[96,512]{1,0:T(8,128)(2,1)S(1)}, u32[]{:S(2)}, u32[]{:S(2)}) collective-permute-start(bf16[96,512]{1,0:T(8,128)(2,1)S(1)} %get-tuple-element.73), channel_id=1, source_target_pairs={{0,12},{4,8},{8,4},{12,0},{16,28},{20,24},{24,20},{28,16},{1,13},{... | collective-permute-start | bytes 294920 | tf_op jit(solution)/shard_map/ppermute | solution.py:29
  7.0 12.6 %collective-permute-start.3 = (bf16[96,512]{1,0:T(8,128)(2,1)S(1)}, bf16[96,512]{1,0:T(8,128)(2,1)S(1)}, u32[]{:S(2)}, u32[]{:S(2)}) collective-permute-start(bf16[96,512]{1,0:T(8,128)(2,1)S(1)} %get-tuple-element.72), channel_id=1, source_target_pairs={{0,16},{4,20},{8,24},{12,28},{16,0},{20,4},{24,8},{28,12},{1,17},{... | collective-permute-start | bytes 294920 | tf_op jit(solution)/shard_map/ppermute | solution.py:29
  10.0 15.2 %collective-permute-start.4 = (bf16[96,512]{1,0:T(8,128)(2,1)S(1)}, bf16[96,512]{1,0:T(8,128)(2,1)S(1)}, u32[]{:S(2)}, u32[]{:S(2)}) collective-permute-start(bf16[96,512]{1,0:T(8,128)(2,1)S(1)} %get-tuple-element.71), channel_id=1, source_target_pairs={{0,20},{4,16},{8,28},{12,24},{16,4},{20,0},{24,12},{28,8},{1,21},{... | collective-permute-start | bytes 294920 | tf_op jit(solution)/shard_map/ppermute | solution.py:29
  13.4 11.9 %collective-permute-start.5 = (bf16[96,512]{1,0:T(8,128)(2,1)S(1)}, bf16[96,512]{1,0:T(8,128)(2,1)S(1)}, u32[]{:S(2)}, u32[]{:S(2)}) collective-permute-start(bf16[96,512]{1,0:T(8,128)(2,1)S(1)} %get-tuple-element.70), channel_id=1, source_target_pairs={{0,24},{4,28},{8,16},{12,20},{16,8},{20,12},{24,0},{28,4},{1,25},{... | collective-permute-start | bytes 294920 | tf_op jit(solution)/shard_map/ppermute | solution.py:29
  17.0 8.2 %collective-permute-start.6 = (bf16[96,512]{1,0:T(8,128)(2,1)S(1)}, bf16[96,512]{1,0:T(8,128)(2,1)S(1)}, u32[]{:S(2)}, u32[]{:S(2)}) collective-permute-start(bf16[96,512]{1,0:T(8,128)(2,1)S(1)} %get-tuple-element.69), channel_id=1, source_target_pairs={{0,28},{4,24},{8,20},{12,16},{16,12},{20,8},{24,4},{28,0},{1,29},{... | collective-permute-start | bytes 294920 | tf_op jit(solution)/shard_map/ppermute | solution.py:29
  17.9 16.9 %collective-permute-start.10 = (bf16[96,512]{1,0:T(8,128)(2,1)S(1)}, bf16[96,512]{1,0:T(8,128)(2,1)S(1)}, u32[]{:S(2)}, u32[]{:S(2)}) collective-permute-start(bf16[96,512]{1,0:T(8,128)(2,1)S(1)} %get-tuple-element.68), channel_id=1, source_target_pairs={{0,4},{4,0},{8,12},{12,8},{16,20},{20,16},{24,28},{28,24},{1,5},{5... | collective-permute-start | bytes 294920 | tf_op jit(solution)/shard_map/ppermute | solution.py:29
  19.6 16.0 %collective-permute-start.11 = (bf16[96,512]{1,0:T(8,128)(2,1)S(1)}, bf16[96,512]{1,0:T(8,128)(2,1)S(1)}, u32[]{:S(2)}, u32[]{:S(2)}) collective-permute-start(bf16[96,512]{1,0:T(8,128)(2,1)S(1)} %get-tuple-element.67), channel_id=1, source_target_pairs={{0,8},{4,12},{8,0},{12,4},{16,24},{20,28},{24,16},{28,20},{1,9},{5... | collective-permute-start | bytes 294920 | tf_op jit(solution)/shard_map/ppermute | solution.py:29
  25.2 11.4 %collective-permute-start.12 = (bf16[96,512]{1,0:T(8,128)(2,1)}, bf16[96,512]{1,0:T(8,128)(2,1)S(1)}, u32[]{:S(2)}, u32[]{:S(2)}) collective-permute-start(bf16[96,512]{1,0:T(8,128)(2,1)} %get-tuple-element.66), channel_id=1, source_target_pairs={{0,12},{4,8},{8,4},{12,0},{16,28},{20,24},{24,20},{28,16},{1,13},{... | collective-permute-start | bytes 294920 | tf_op jit(solution)/shard_map/ppermute | solution.py:29
  28.2 23.4 %copy-start.4 = (bf16[8,96,512]{2,1,0:T(8,128)(2,1)S(1)}, bf16[8,96,512]{2,1,0:T(8,128)(2,1)}, u32[]{:S(2)}) copy-start(bf16[8,96,512]{2,1,0:T(8,128)(2,1)} %shard_map.171) | copy-start | bytes 2359300
  28.2 41.7 %copy-start.1 = (bf16[1,256,2048]{2,1,0:T(8,128)(2,1)S(1)}, bf16[1,256,2048]{2,1,0:T(8,128)(2,1)}, u32[]{:S(2)}) copy-start(bf16[1,256,2048]{2,1,0:T(8,128)(2,1)} %param.22) | copy-start | bytes 3145732
  28.2 24.0 %collective-permute-start.8 = (bf16[768,512]{1,0:T(8,128)(2,1)}, bf16[768,512]{1,0:T(8,128)(2,1)}, u32[]{:S(2)}, u32[]{:S(2)}) collective-permute-start(bf16[768,512]{1,0:T(8,128)(2,1)} %bitcast.52), channel_id=1, source_target_pairs={{0,2},{1,3},{2,0},{3,1},{4,6},{5,7},{6,4},{7,5},{8,10},{9,11},{10,... | collective-permute-start | bytes 2359304 | tf_op jit(solution)/shard_map/ppermute | solution.py:29
  29.7 16.6 %collective-permute-start.13 = (bf16[96,512]{1,0:T(8,128)(2,1)}, bf16[96,512]{1,0:T(8,128)(2,1)S(1)}, u32[]{:S(2)}, u32[]{:S(2)}) collective-permute-start(bf16[96,512]{1,0:T(8,128)(2,1)} %get-tuple-element.65), channel_id=1, source_target_pairs={{0,16},{4,20},{8,24},{12,28},{16,0},{20,4},{24,8},{28,12},{1,17},{... | collective-permute-start | bytes 294920 | tf_op jit(solution)/shard_map/ppermute | solution.py:29
  34.8 13.4 %collective-permute-start.14 = (bf16[96,512]{1,0:T(8,128)(2,1)}, bf16[96,512]{1,0:T(8,128)(2,1)S(1)}, u32[]{:S(2)}, u32[]{:S(2)}) collective-permute-start(bf16[96,512]{1,0:T(8,128)(2,1)} %get-tuple-element.64), channel_id=1, source_target_pairs={{0,20},{4,16},{8,28},{12,24},{16,4},{20,0},{24,12},{28,8},{1,21},{... | collective-permute-start | bytes 294920 | tf_op jit(solution)/shard_map/ppermute | solution.py:29
  35.6 12.5 %collective-permute-start.15 = (bf16[96,512]{1,0:T(8,128)(2,1)}, bf16[96,512]{1,0:T(8,128)(2,1)S(1)}, u32[]{:S(2)}, u32[]{:S(2)}) collective-permute-start(bf16[96,512]{1,0:T(8,128)(2,1)} %get-tuple-element.63), channel_id=1, source_target_pairs={{0,24},{4,28},{8,16},{12,20},{16,8},{20,12},{24,0},{28,4},{1,25},{... | collective-permute-start | bytes 294920 | tf_op jit(solution)/shard_map/ppermute | solution.py:29
  36.6 11.6 %collective-permute-start.16 = (bf16[96,512]{1,0:T(8,128)(2,1)}, bf16[96,512]{1,0:T(8,128)(2,1)}, u32[]{:S(2)}, u32[]{:S(2)}) collective-permute-start(bf16[96,512]{1,0:T(8,128)(2,1)} %get-tuple-element.62), channel_id=1, source_target_pairs={{0,28},{4,24},{8,20},{12,16},{16,12},{20,8},{24,4},{28,0},{1,29},{... | collective-permute-start | bytes 294920 | tf_op jit(solution)/shard_map/ppermute | solution.py:29
  51.1 18.2 %collective-permute-start.18 = (bf16[768,512]{1,0:T(8,128)(2,1)}, bf16[768,512]{1,0:T(8,128)(2,1)}, u32[]{:S(2)}, u32[]{:S(2)}) collective-permute-start(bf16[768,512]{1,0:T(8,128)(2,1)} %bitcast.56), channel_id=1, source_target_pairs={{0,2},{1,3},{2,0},{3,1},{4,6},{5,7},{6,4},{7,5},{8,10},{9,11},{10,... | collective-permute-start | bytes 2359304 | tf_op jit(solution)/shard_map/ppermute | solution.py:29
  51.7 18.3 %collective-permute-start.17 = (bf16[768,512]{1,0:T(8,128)(2,1)}, bf16[768,512]{1,0:T(8,128)(2,1)}, u32[]{:S(2)}, u32[]{:S(2)}) collective-permute-start(bf16[768,512]{1,0:T(8,128)(2,1)} %bitcast.57), channel_id=1, source_target_pairs={{0,1},{1,0},{2,3},{3,2},{4,5},{5,4},{6,7},{7,6},{8,9},{9,8},{10,11... | collective-permute-start | bytes 2359304 | tf_op jit(solution)/shard_map/ppermute | solution.py:29
  51.7 21.1 %collective-permute-start.7 = (bf16[768,512]{1,0:T(8,128)(2,1)S(1)}, bf16[768,512]{1,0:T(8,128)(2,1)}, u32[]{:S(2)}, u32[]{:S(2)}) collective-permute-start(bf16[768,512]{1,0:T(8,128)(2,1)S(1)} %bitcast.55), channel_id=1, source_target_pairs={{0,1},{1,0},{2,3},{3,2},{4,5},{5,4},{6,7},{7,6},{8,9},{9,8},{10,11... | collective-permute-start | bytes 2359304 | tf_op jit(solution)/shard_map/ppermute | solution.py:29
  52.2 20.6 %collective-permute-start.9 = (bf16[768,512]{1,0:T(8,128)(2,1)}, bf16[768,512]{1,0:T(8,128)(2,1)}, u32[]{:S(2)}, u32[]{:S(2)}) collective-permute-start(bf16[768,512]{1,0:T(8,128)(2,1)} %collective-permute-done.8.refs_2_), channel_id=1, source_target_pairs={{0,1},{1,0},{2,3},{3,2},{4,5},{5,4},{6,7},{7,6},{8,9},{9,8},{10,11... | collective-permute-start | bytes 2359304 | tf_op jit(solution)/shard_map/ppermute | solution.py:29
  52.3 19.2 %copy-start.5 = (bf16[8,96,512]{2,1,0:T(8,128)(2,1)S(1)}, bf16[8,96,512]{2,1,0:T(8,128)(2,1)}, u32[]{:S(2)}) copy-start(bf16[8,96,512]{2,1,0:T(8,128)(2,1)} %shard_map.172) | copy-start | bytes 2359300
  69.3 9.7 %collective-permute-start.19 = (bf16[768,512]{1,0:T(8,128)(2,1)}, bf16[768,512]{1,0:T(8,128)(2,1)}, u32[]{:S(2)}, u32[]{:S(2)}) collective-permute-start(bf16[768,512]{1,0:T(8,128)(2,1)} %collective-permute-done.18.refs_0_.refs_6_), channel_id=1, source_target_pairs={{0,1},{1,0},{2,3},{3,2},{4,5},{5,4},{6,7},{7,6},{8,9},{9,8},{10,11... | collective-permute-start | bytes 2359304 | tf_op jit(solution)/shard_map/ppermute | solution.py:29
  86.6 23.9 %copy-start.11 = (bf16[768,512]{1,0:T(8,128)(2,1)S(1)}, bf16[768,512]{1,0:T(8,128)(2,1)}, u32[]{:S(2)}) copy-start(bf16[768,512]{1,0:T(8,128)(2,1)} %get-tuple-element.37) | copy-start | bytes 2359300
  86.6 2.7 %collective-permute-start.21 = (bf16[768,512]{1,0:T(8,128)(2,1)}, bf16[768,512]{1,0:T(8,128)(2,1)S(1)}, u32[]{:S(2)}, u32[]{:S(2)}) collective-permute-start(bf16[768,512]{1,0:T(8,128)(2,1)} %get-tuple-element.40), channel_id=1, source_target_pairs={{0,1},{1,0},{2,3},{3,2},{4,5},{5,4},{6,7},{7,6},{8,9},{9,8},{10,11... | collective-permute-start | bytes 2359304 | tf_op jit(solution)/shard_map/ppermute | solution.py:29
  87.2 4.1 %collective-permute-start.20 = (bf16[768,512]{1,0:T(8,128)(2,1)}, bf16[768,512]{1,0:T(8,128)(2,1)S(1)}, u32[]{:S(2)}, u32[]{:S(2)}) collective-permute-start(bf16[768,512]{1,0:T(8,128)(2,1)} %get-tuple-element.38), channel_id=1, source_target_pairs={{0,1},{1,0},{2,3},{3,2},{4,5},{5,4},{6,7},{7,6},{8,9},{9,8},{10,11... | collective-permute-start | bytes 2359304 | tf_op jit(solution)/shard_map/ppermute | solution.py:29
  90.6 19.9 %collective-permute-start.22 = (bf16[768,512]{1,0:T(8,128)(2,1)S(1)}, bf16[768,512]{1,0:T(8,128)(2,1)S(1)}, u32[]{:S(2)}, u32[]{:S(2)}) collective-permute-start(bf16[768,512]{1,0:T(8,128)(2,1)S(1)} %add_convert_fusion.1), channel_id=1, source_target_pairs={{0,2},{1,3},{2,0},{3,1},{4,6},{5,7},{6,4},{7,5},{8,10},{9,11},{10,... | collective-permute-start | bytes 2359304 | tf_op jit(solution)/shard_map/ppermute | solution.py:29
  110.9 28.0 %copy-start.2 = (bf16[768,512]{1,0:T(8,128)(2,1)}, bf16[768,512]{1,0:T(8,128)(2,1)S(1)}, u32[]{:S(2)}) copy-start(bf16[768,512]{1,0:T(8,128)(2,1)S(1)} %add_convert_fusion) | copy-start | bytes 2359300
  110.9 15.3 %copy-start.15 = (bf16[256,512]{1,0:T(8,128)(2,1)S(1)}, bf16[256,512]{1,0:T(8,128)(2,1)}, u32[]{:S(2)}) copy-start(bf16[256,512]{1,0:T(8,128)(2,1)} %param.14) | copy-start | bytes 786436
  111.6 31.0 %copy-start.10 = (bf16[256,512]{1,0:T(8,128)(2,1)S(1)}, bf16[256,512]{1,0:T(8,128)(2,1)}, u32[]{:S(2)}) copy-start(bf16[256,512]{1,0:T(8,128)(2,1)} %value_ref.3) | copy-start | bytes 786436
  111.6 31.0 %copy-start.12 = (bf16[256,256]{1,0:T(8,128)(2,1)S(1)}, bf16[256,256]{1,0:T(8,128)(2,1)}, u32[]{:S(2)}) copy-start(bf16[256,256]{1,0:T(8,128)(2,1)} %key_ref.3) | copy-start | bytes 393220
  111.6 10.7 %collective-permute-start.23 = (bf16[96,512]{1,0:T(8,128)(2,1)S(1)}, bf16[96,512]{1,0:T(8,128)(2,1)S(1)}, u32[]{:S(2)}, u32[]{:S(2)}) collective-permute-start(bf16[96,512]{1,0:T(8,128)(2,1)S(1)} %get-tuple-element.61), channel_id=1, source_target_pairs={{0,4},{4,0},{8,12},{12,8},{16,20},{20,16},{24,28},{28,24},{1,5},{5... | collective-permute-start | bytes 294920 | tf_op jit(solution)/shard_map/ppermute | solution.py:29
  113.0 11.7 %collective-permute-start.24 = (bf16[96,512]{1,0:T(8,128)(2,1)S(1)}, bf16[96,512]{1,0:T(8,128)(2,1)S(1)}, u32[]{:S(2)}, u32[]{:S(2)}) collective-permute-start(bf16[96,512]{1,0:T(8,128)(2,1)S(1)} %get-tuple-element.60), channel_id=1, source_target_pairs={{0,8},{4,12},{8,0},{12,4},{16,24},{20,28},{24,16},{28,20},{1,9},{5... | collective-permute-start | bytes 294920 | tf_op jit(solution)/shard_map/ppermute | solution.py:29
  118.3 7.9 %collective-permute-start.25 = (bf16[96,512]{1,0:T(8,128)(2,1)S(1)}, bf16[96,512]{1,0:T(8,128)(2,1)}, u32[]{:S(2)}, u32[]{:S(2)}) collective-permute-start(bf16[96,512]{1,0:T(8,128)(2,1)S(1)} %get-tuple-element.59), channel_id=1, source_target_pairs={{0,12},{4,8},{8,4},{12,0},{16,28},{20,24},{24,20},{28,16},{1,13},{... | collective-permute-start | bytes 294920 | tf_op jit(solution)/shard_map/ppermute | solution.py:29
  118.5 12.7 %collective-permute-start.26 = (bf16[96,512]{1,0:T(8,128)(2,1)S(1)}, bf16[96,512]{1,0:T(8,128)(2,1)}, u32[]{:S(2)}, u32[]{:S(2)}) collective-permute-start(bf16[96,512]{1,0:T(8,128)(2,1)S(1)} %get-tuple-element.58), channel_id=1, source_target_pairs={{0,16},{4,20},{8,24},{12,28},{16,0},{20,4},{24,8},{28,12},{1,17},{... | collective-permute-start | bytes 294920 | tf_op jit(solution)/shard_map/ppermute | solution.py:29
  121.3 14.9 %collective-permute-start.27 = (bf16[96,512]{1,0:T(8,128)(2,1)S(1)}, bf16[96,512]{1,0:T(8,128)(2,1)}, u32[]{:S(2)}, u32[]{:S(2)}) collective-permute-start(bf16[96,512]{1,0:T(8,128)(2,1)S(1)} %get-tuple-element.57), channel_id=1, source_target_pairs={{0,20},{4,16},{8,28},{12,24},{16,4},{20,0},{24,12},{28,8},{1,21},{... | collective-permute-start | bytes 294920 | tf_op jit(solution)/shard_map/ppermute | solution.py:29
  122.3 16.5 %copy-start.23 = (bf16[96,512]{1,0:T(8,128)(2,1)}, bf16[96,512]{1,0:T(8,128)(2,1)S(1)}, u32[]{:S(2)}) copy-start(bf16[96,512]{1,0:T(8,128)(2,1)S(1)} %collective-permute-done.23.refs_0_) | copy-start | bytes 294916
  122.3 16.5 %collective-permute-start.28 = (bf16[96,512]{1,0:T(8,128)(2,1)}, bf16[96,512]{1,0:T(8,128)(2,1)}, u32[]{:S(2)}, u32[]{:S(2)}) collective-permute-start(bf16[96,512]{1,0:T(8,128)(2,1)} %get-tuple-element.56), channel_id=1, source_target_pairs={{0,24},{4,28},{8,16},{12,20},{16,8},{20,12},{24,0},{28,4},{1,25},{... | collective-permute-start | bytes 294920 | tf_op jit(solution)/shard_map/ppermute | solution.py:29
  124.7 14.2 %copy-start.24 = (bf16[96,512]{1,0:T(8,128)(2,1)}, bf16[96,512]{1,0:T(8,128)(2,1)S(1)}, u32[]{:S(2)}) copy-start(bf16[96,512]{1,0:T(8,128)(2,1)S(1)} %collective-permute-done.24.refs_1_) | copy-start | bytes 294916
  124.7 14.1 %collective-permute-start.29 = (bf16[96,512]{1,0:T(8,128)(2,1)}, bf16[96,512]{1,0:T(8,128)(2,1)}, u32[]{:S(2)}, u32[]{:S(2)}) collective-permute-start(bf16[96,512]{1,0:T(8,128)(2,1)} %get-tuple-element.55), channel_id=1, source_target_pairs={{0,28},{4,24},{8,20},{12,16},{16,12},{20,8},{24,4},{28,0},{1,29},{... | collective-permute-start | bytes 294920 | tf_op jit(solution)/shard_map/ppermute | solution.py:29
  126.2 46.0 %collective-permute-start.46 = (bf16[256,512]{1,0:T(8,128)(2,1)S(1)}, bf16[256,512]{1,0:T(8,128)(2,1)S(1)}, u32[]{:S(2)}, u32[]{:S(2)}) collective-permute-start(bf16[256,512]{1,0:T(8,128)(2,1)S(1)} %copy-done.15), channel_id=1, source_target_pairs={{0,8},{4,12},{8,0},{12,4},{16,24},{20,28},{24,16},{28,20},{1,9},{5... | collective-permute-start | bytes 786440 | tf_op jit(solution)/shard_map/ppermute | solution.py:29
  131.2 41.0 %collective-permute-start.47 = (bf16[256,512]{1,0:T(8,128)(2,1)S(1)}, bf16[256,512]{1,0:T(8,128)(2,1)S(1)}, u32[]{:S(2)}, u32[]{:S(2)}) collective-permute-start(bf16[256,512]{1,0:T(8,128)(2,1)S(1)} %copy-done.15), channel_id=1, source_target_pairs={{0,16},{4,20},{8,24},{12,28},{16,0},{20,4},{24,8},{28,12},{1,17},{... | collective-permute-start | bytes 786440 | tf_op jit(solution)/shard_map/ppermute | solution.py:29
  136.2 36.0 %collective-permute-start.48 = (bf16[256,512]{1,0:T(8,128)(2,1)S(1)}, bf16[256,512]{1,0:T(8,128)(2,1)S(1)}, u32[]{:S(2)}, u32[]{:S(2)}) collective-permute-start(bf16[256,512]{1,0:T(8,128)(2,1)S(1)} %copy-done.15), channel_id=1, source_target_pairs={{0,24},{4,28},{8,16},{12,20},{16,8},{20,12},{24,0},{28,4},{1,25},{... | collective-permute-start | bytes 786440 | tf_op jit(solution)/shard_map/ppermute | solution.py:29
  141.8 6.6 %collective-permute-start.31 = (bf16[256,512]{1,0:T(8,128)(2,1)}, bf16[256,512]{1,0:T(8,128)(2,1)S(1)}, u32[]{:S(2)}, u32[]{:S(2)}) collective-permute-start(bf16[256,512]{1,0:T(8,128)(2,1)} %shard_map.176.refs_0_), channel_id=1, source_target_pairs={{0,2},{1,3},{2,0},{3,1},{4,6},{5,7},{6,4},{7,5},{8,10},{9,11},{10,... | collective-permute-start | bytes 786440 | tf_op jit(solution)/shard_map/ppermute | solution.py:29
  143.0 7.9 %collective-permute-start.30 = (bf16[256,512]{1,0:T(8,128)(2,1)}, bf16[256,512]{1,0:T(8,128)(2,1)S(1)}, u32[]{:S(2)}, u32[]{:S(2)}) collective-permute-start(bf16[256,512]{1,0:T(8,128)(2,1)} %shard_map.176.refs_0_), channel_id=1, source_target_pairs={{0,1},{1,0},{2,3},{3,2},{4,5},{5,4},{6,7},{7,6},{8,9},{9,8},{10,11... | collective-permute-start | bytes 786440 | tf_op jit(solution)/shard_map/ppermute | solution.py:29
  148.4 2.7 %collective-permute-start.32 = (bf16[256,512]{1,0:T(8,128)(2,1)S(1)}, bf16[256,512]{1,0:T(8,128)(2,1)}, u32[]{:S(2)}, u32[]{:S(2)}) collective-permute-start(bf16[256,512]{1,0:T(8,128)(2,1)S(1)} %collective-permute-done.31.refs_2_), channel_id=1, source_target_pairs={{0,1},{1,0},{2,3},{3,2},{4,5},{5,4},{6,7},{7,6},{8,9},{9,8},{10,11... | collective-permute-start | bytes 786440 | tf_op jit(solution)/shard_map/ppermute | solution.py:29
  150.8 22.2 %copy-start.16 = (bf16[256,512]{1,0:T(8,128)(2,1)S(1)}, bf16[256,512]{1,0:T(8,128)(2,1)}, u32[]{:S(2)}) copy-start(bf16[256,512]{1,0:T(8,128)(2,1)} %param.14) | copy-start | bytes 786436
  150.8 25.7 %collective-permute-start.38 = (bf16[128,512]{1,0:T(8,128)(2,1)}, bf16[128,512]{1,0:T(8,128)(2,1)}, u32[]{:S(2)}, u32[]{:S(2)}) collective-permute-start(bf16[128,512]{1,0:T(8,128)(2,1)} %constant_dynamic-slice_fusion), channel_id=1, source_target_pairs={{0,4},{4,0},{8,12},{12,8},{16,20},{20,16},{24,28},{28,24},{1,5},{5... | collective-permute-start | bytes 393224 | tf_op jit(solution)/shard_map/ppermute | solution.py:29
  155.1 49.0 %copy-start.13 = (bf16[128,512]{1,0:T(8,128)(2,1)S(1)}, bf16[128,512]{1,0:T(8,128)(2,1)}, u32[]{:S(2)}) copy-start(bf16[128,512]{1,0:T(8,128)(2,1)} %get-tuple-element.42) | copy-start | bytes 393220
  155.1 48.4 %all-to-all-start = ((bf16[8,64,256]{2,1,0:T(8,128)(2,1)}), bf16[8,64,256]{2,1,0:T(8,128)(2,1)}, u32[]{:S(2)}, u32[]{:S(2)}) async-start(bf16[8,64,256]{2,1,0:T(8,128)(2,1)} %get-tuple-element.46), calls=%async_computation | async-start | bytes 524288 | tf_op jit(solution)/shard_map/all_to_all | solution.py:43
  174.3 57.6 %copy-start.3 = (bf16[4,256,512]{2,1,0:T(8,128)(2,1)}, bf16[4,256,512]{2,1,0:T(8,128)(2,1)S(1)}, u32[]{:S(2)}) copy-start(bf16[4,256,512]{2,1,0:T(8,128)(2,1)S(1)} %pad_maximum_fusion.refs_4_) | copy-start | bytes 3145732
  174.3 60.3 %collective-permute-start.49 = (bf16[4,256,512]{2,1,0:T(8,128)(2,1)S(1)}, bf16[4,256,512]{2,1,0:T(8,128)(2,1)S(1)}, u32[]{:S(2)}, u32[]{:S(2)}) collective-permute-start(bf16[4,256,512]{2,1,0:T(8,128)(2,1)S(1)} %pad_maximum_fusion.refs_4_), channel_id=1, source_target_pairs={{0,4},{4,0},{8,12},{12,8},{16,20},{20,16},{24,28},{28,24},{1,5},{5... | collective-permute-start | bytes 3145736 | tf_op jit(solution)/shard_map/ppermute | solution.py:29
  176.4 27.1 %collective-permute-start.33 = (bf16[128,512]{1,0:T(8,128)(2,1)S(1)}, bf16[128,512]{1,0:T(8,128)(2,1)}, u32[]{:S(2)}, u32[]{:S(2)}) collective-permute-start(bf16[128,512]{1,0:T(8,128)(2,1)S(1)} %copy-done.39), channel_id=1, source_target_pairs={{0,4},{4,0},{8,12},{12,8},{16,20},{20,16},{24,28},{28,24},{1,5},{5... | collective-permute-start | bytes 393224 | tf_op jit(solution)/shard_map/ppermute | solution.py:29
  178.1 26.9 %collective-permute-start.39 = (bf16[128,512]{1,0:T(8,128)(2,1)}, bf16[128,512]{1,0:T(8,128)(2,1)}, u32[]{:S(2)}, u32[]{:S(2)}) collective-permute-start(bf16[128,512]{1,0:T(8,128)(2,1)} %fusion.16), channel_id=1, source_target_pairs={{0,8},{4,12},{8,16},{12,20},{16,24},{20,28},{1,9},{5,13},{9,17},{1... | collective-permute-start | bytes 393224 | tf_op jit(solution)/shard_map/ppermute | solution.py:326
  182.6 23.7 %collective-permute-start.40 = (bf16[128,512]{1,0:T(8,128)(2,1)}, bf16[128,512]{1,0:T(8,128)(2,1)}, u32[]{:S(2)}, u32[]{:S(2)}) collective-permute-start(bf16[128,512]{1,0:T(8,128)(2,1)} %fusion.16), channel_id=1, source_target_pairs={{0,16},{4,20},{8,24},{12,28},{1,17},{5,21},{9,25},{13,29},{2,18},{... | collective-permute-start | bytes 393224 | tf_op jit(solution)/shard_map/ppermute | solution.py:326
  186.9 20.8 %collective-permute-start.41 = (bf16[128,512]{1,0:T(8,128)(2,1)}, bf16[128,512]{1,0:T(8,128)(2,1)}, u32[]{:S(2)}, u32[]{:S(2)}) collective-permute-start(bf16[128,512]{1,0:T(8,128)(2,1)} %fusion.16), channel_id=1, source_target_pairs={{0,24},{4,28},{1,25},{5,29},{2,26},{6,30},{3,27},{7,31}} | collective-permute-start | bytes 393224 | tf_op jit(solution)/shard_map/ppermute | solution.py:326
  203.5 17.3 %collective-permute-start.44 = (bf16[8,64,256]{2,1,0:T(8,128)(2,1)}, bf16[8,64,256]{2,1,0:T(8,128)(2,1)}, u32[]{:S(2)}, u32[]{:S(2)}) collective-permute-start(bf16[8,64,256]{2,1,0:T(8,128)(2,1)} %all-to-all-done.refs_0_), channel_id=1, source_target_pairs={{0,2},{1,3},{2,0},{3,1},{4,6},{5,7},{6,4},{7,5},{8,10},{9,11},{10,... | collective-permute-start | bytes 786440 | tf_op jit(solution)/shard_map/ppermute | solution.py:29
  205.0 8.0 %collective-permute-start.34 = (bf16[128,512]{1,0:T(8,128)(2,1)S(1)}, bf16[128,512]{1,0:T(8,128)(2,1)S(1)}, u32[]{:S(2)}, u32[]{:S(2)}) collective-permute-start(bf16[128,512]{1,0:T(8,128)(2,1)S(1)} %fusion.14), channel_id=1, source_target_pairs={{8,0},{12,4},{16,8},{20,12},{24,16},{28,20},{9,1},{13,5},{17,9},{2... | collective-permute-start | bytes 393224 | tf_op jit(solution)/shard_map/ppermute | solution.py:326
  206.3 14.5 %collective-permute-start.35 = (bf16[128,512]{1,0:T(8,128)(2,1)S(1)}, bf16[128,512]{1,0:T(8,128)(2,1)S(1)}, u32[]{:S(2)}, u32[]{:S(2)}) collective-permute-start(bf16[128,512]{1,0:T(8,128)(2,1)S(1)} %fusion.14), channel_id=1, source_target_pairs={{16,0},{20,4},{24,8},{28,12},{17,1},{21,5},{25,9},{29,13},{18,2},{... | collective-permute-start | bytes 393224 | tf_op jit(solution)/shard_map/ppermute | solution.py:326
  207.6 13.7 %collective-permute-start.36 = (bf16[128,512]{1,0:T(8,128)(2,1)S(1)}, bf16[128,512]{1,0:T(8,128)(2,1)S(1)}, u32[]{:S(2)}, u32[]{:S(2)}) collective-permute-start(bf16[128,512]{1,0:T(8,128)(2,1)S(1)} %fusion.14), channel_id=1, source_target_pairs={{24,0},{28,4},{25,1},{29,5},{26,2},{30,6},{27,3},{31,7}} | collective-permute-start | bytes 393224 | tf_op jit(solution)/shard_map/ppermute | solution.py:326
  213.0 18.9 %collective-permute-start.42 = (bf16[128,512]{1,0:T(8,128)(2,1)}, bf16[128,512]{1,0:T(8,128)(2,1)}, u32[]{:S(2)}, u32[]{:S(2)}) collective-permute-start(bf16[128,512]{1,0:T(8,128)(2,1)} %get-tuple-element.53), channel_id=1, source_target_pairs={{0,4},{4,0},{8,12},{12,8},{16,20},{20,16},{24,28},{28,24},{1,5},{5... | collective-permute-start | bytes 393224 | tf_op jit(solution)/shard_map/ppermute | solution.py:29
  220.8 13.8 %collective-permute-start.43 = (bf16[8,64,256]{2,1,0:T(8,128)(2,1)}, bf16[8,64,256]{2,1,0:T(8,128)(2,1)S(1)}, u32[]{:S(2)}, u32[]{:S(2)}) collective-permute-start(bf16[8,64,256]{2,1,0:T(8,128)(2,1)} %all-to-all-done.refs_0_), channel_id=1, source_target_pairs={{0,1},{1,0},{2,3},{3,2},{4,5},{5,4},{6,7},{7,6},{8,9},{9,8},{10,11... | collective-permute-start | bytes 786440 | tf_op jit(solution)/shard_map/ppermute | solution.py:29
  220.8 13.8 %collective-permute-start.45 = (bf16[8,64,256]{2,1,0:T(8,128)(2,1)}, bf16[8,64,256]{2,1,0:T(8,128)(2,1)}, u32[]{:S(2)}, u32[]{:S(2)}) collective-permute-start(bf16[8,64,256]{2,1,0:T(8,128)(2,1)} %collective-permute-done.44.refs_2_), channel_id=1, source_target_pairs={{0,1},{1,0},{2,3},{3,2},{4,5},{5,4},{6,7},{7,6},{8,9},{9,8},{10,11... | collective-permute-start | bytes 786440 | tf_op jit(solution)/shard_map/ppermute | solution.py:29
  223.1 11.5 %collective-permute-start.37 = (bf16[128,512]{1,0:T(8,128)(2,1)}, bf16[128,512]{1,0:T(8,128)(2,1)S(1)}, u32[]{:S(2)}, u32[]{:S(2)}) collective-permute-start(bf16[128,512]{1,0:T(8,128)(2,1)} %get-tuple-element.76), channel_id=1, source_target_pairs={{0,4},{4,0},{8,12},{12,8},{16,20},{20,16},{24,28},{28,24},{1,5},{5... | collective-permute-start | bytes 393224 | tf_op jit(solution)/shard_map/ppermute | solution.py:29
  (27 other events, 115.4 us)
